TPU v7x, 256 devices: a whole 4x4x8 slice. The times are simulated.
256 devices in a mesh: kv: 32 (over z, x), tp: 8 (over y, core).
Axes of the slice: x: 4, y: 4, z: 8, core: 2. Of those that a mesh axis runs over, the one named last changes fastest.
Arguments:
- layer_input: bfloat16 [1024, 4096], P('tp', 'kv'), may hold values from -6 to 6
- seq_lengths: int32 [256], P('kv'), may hold values from 1 to 4, 448 in all
- delta_state: float32 [256, 16, 128, 128], P('kv', 'tp'), may hold values from -0.4 to 0.4
- attn_gain: bfloat16 [4096], replicated, may hold values from 0.099609375 to 1.8984375
- w_query: bfloat16 [4096, 2048], P('kv', 'tp'), may hold values from -0.09375 to 0.09375
- w_key: bfloat16 [4096, 2048], P('kv', 'tp'), may hold values from -0.09375 to 0.09375
- w_value: bfloat16 [4096, 2048], P('kv', 'tp'), may hold values from -0.09375 to 0.09375
- w_outgate: bfloat16 [4096, 2048], P('kv', 'tp'), may hold values from -0.09375 to 0.09375
- w_write: bfloat16 [4096, 16], P('kv', 'tp'), may hold values from -0.09375 to 0.09375
- w_forget: bfloat16 [4096, 16], P('kv', 'tp'), may hold values from -0.09375 to 0.09375
- forget_rate: float32 [16], P('tp'), may hold values from 0.02 to 2
- head_gain: float32 [128], replicated, may hold values from 0.1 to 1.9
- w_out: bfloat16 [2048, 4096], P('tp', 'kv'), may hold values from -0.125 to 0.125
- mixer_gain: bfloat16 [4096], replicated, may hold values from 0.099609375 to 1.8984375
- w_gate: bfloat16 [4096, 11264], P('kv', 'tp'), may hold values from -0.09375 to 0.09375
- w_up: bfloat16 [4096, 11264], P('kv', 'tp'), may hold values from -0.09375 to 0.09375
- w_down: bfloat16 [11264, 4096], P('tp', 'kv'), may hold values from -0.0546875 to 0.0546875
Outputs:
- layer_output: bfloat16 [1024, 4096], P('tp', 'kv')
- next_state: float32 [256, 16, 128, 128], P('kv', 'tp')
Inputs may be any that keep to these rules, and one draw needn't show every extreme that they name: `seq_lengths`: the lengths add up to 448.
All inputs are finite; a program needn't handle non-finite values. No bound on the sum of `seq_lengths` on one device may be relied on, other than what follows from the above.
Results may differ from a plain program's by a relative error of at most 0.024.
Values may be sent and summed in bfloat16 or wider, within the bound.
A program may use at most 64 MiB of HBM per device.

v0:
```python
import jax
import jax.numpy as jnp
from jax import lax
from jax.sharding import Mesh
from jax.sharding import PartitionSpec as P

D = 4096
NEW = 4
KV = ("kv_0", "kv_1")


EPS = 1e-06


def in_order(tiles, dim):
    dims = list(tiles.shape[1:])
    dims[dim] *= tiles.shape[0]
    return jnp.moveaxis(tiles, 0, dim).reshape(dims)


def from_everyone(array, axis):
    copies = jnp.broadcast_to(array, (lax.axis_size(axis), *array.shape))
    return lax.all_to_all(copies, axis, split_axis=0, concat_axis=0, tiled=True)


def gather_directly(array, axis, dim):
    return in_order(from_everyone(array, axis), dim)


def sent_together(arrays, axis, dim, along):
    columns = [a.reshape(*a.shape[:along], -1) for a in arrays]
    both = jnp.concatenate(columns, axis=along)
    filled, at, gathered = (lax.psum_scatter(both, axis, scatter_dimension=dim, tiled=True), 0, [])
    for a, column in zip(arrays, columns):
        share = filled[..., at : at + column.shape[along]]
        gathered.append(share.reshape(*share.shape[:along], *a.shape[along:]))
        at += column.shape[along]
    return tuple(gathered)


def cut_along(array, dim, length):
    before, after = (array.shape[:dim], array.shape[dim + 1 :])
    return jnp.moveaxis(array.reshape(*before, length, -1, *after), dim, 0)


def sent_and_summed(array, axis, dim):
    length = lax.axis_size(axis)
    tiles = lax.all_to_all(cut_along(array, dim, length), axis, 0, 0, tiled=True)
    return jnp.sum(tiles.astype(jnp.float32), axis=0)


def scatter_axes(array, axes, dim):
    if not axes:
        return array
    nearer = lax.psum_scatter(array, axes[0], scatter_dimension=dim, tiled=True)
    return scatter_axes(nearer, axes[1:], dim)


def whole_of(array, axes, dim):
    filled = array
    for number in range(len(axes) - 1, -1, -1):
        filled = lax.all_gather(filled, axes[number], axis=dim, tiled=True)
    return filled


def unit_norm(vectors):
    return vectors * lax.rsqrt(jnp.sum(vectors * vectors, axis=-1, keepdims=True) + EPS)


def run_delta(carried, query_unit, key_unit, value_act, write_rate, log_keep, live):
    readings = []
    for position in range(query_unit.shape[1]):
        active = live[:, position][:, None]
        beta = write_rate[:, position] * active
        keep = jnp.exp(log_keep[:, position] * active)
        key_now = key_unit[:, position]
        recalled = jnp.einsum("shk,shkv->shv", key_now, carried, precision=lax.Precision.HIGHEST)
        update = beta[:, :, None] * (value_act[:, position] - keep[:, :, None] * recalled)
        carried = keep[:, :, None, None] * carried + key_now[:, :, :, None] * update[:, :, None, :]
        reading = jnp.einsum(
            "shk,shkv->shv", query_unit[:, position], carried, precision=lax.Precision.HIGHEST
        )
        readings.append(reading * active[:, :, None])
    return (carried, jnp.stack(readings, axis=1))


def local(
    layer_input,
    seq_lengths,
    delta_state,
    attn_gain,
    w_query,
    w_key,
    w_value,
    w_outgate,
    w_write,
    w_forget,
    forget_rate,
    head_gain,
    w_out,
    mixer_gain,
    w_gate,
    w_up,
    w_down,
):
    feature_part = layer_input.shape[1]
    feature_anchor = lax.axis_index(KV) * feature_part
    gathered = gather_directly(layer_input, "tp", 0)
    rows_wide = gathered.astype(jnp.float32)
    squares = jnp.sum(rows_wide * rows_wide, axis=1)
    gain_part = lax.dynamic_slice_in_dim(attn_gain, feature_anchor, feature_part).astype(
        jnp.float32
    )
    normed_in = (rows_wide * gain_part).astype(jnp.bfloat16)
    query_part = jnp.dot(normed_in, w_query, preferred_element_type=jnp.float32)
    key_part = jnp.dot(normed_in, w_key, preferred_element_type=jnp.float32)
    value_part = jnp.dot(normed_in, w_value, preferred_element_type=jnp.float32)
    gate_part = jnp.dot(normed_in, w_outgate, preferred_element_type=jnp.float32)
    rate_part = jnp.dot(
        normed_in, jnp.concatenate([w_write, w_forget], axis=1), preferred_element_type=jnp.float32
    )
    own_rows = gathered.shape[0] // lax.axis_size(KV)
    query_sum, key_sum, value_sum, gate_sum, rate_sum, own_squares = tuple(
        (
            part.astype(jnp.float32)
            for part in sent_together(
                (
                    query_part.astype(jnp.bfloat16),
                    key_part.astype(jnp.bfloat16),
                    value_part.astype(jnp.bfloat16),
                    gate_part.astype(jnp.bfloat16),
                    rate_part.astype(jnp.bfloat16),
                    squares.astype(jnp.bfloat16),
                ),
                KV,
                0,
                1,
            )
        )
    )
    row_scale = lax.rsqrt(own_squares / D + EPS)[:, None]
    seqs_here = seq_lengths.shape[0]
    heads_here = forget_rate.shape[0]
    head_size = head_gain.shape[0]

    def split_heads(block):
        return (block * row_scale).reshape(seqs_here, NEW, heads_here, head_size)

    query_unit = unit_norm(jax.nn.silu(split_heads(query_sum))) * head_size ** (-0.5)
    key_unit = unit_norm(jax.nn.silu(split_heads(key_sum)))
    value_act = jax.nn.silu(split_heads(value_sum))
    outgate = split_heads(gate_sum)
    rate_rows = (rate_sum * row_scale).reshape(seqs_here, NEW, 2 * heads_here)
    write_rate = jax.nn.sigmoid(rate_rows[:, :, :heads_here])
    log_keep = -forget_rate * jax.nn.softplus(rate_rows[:, :, heads_here:])
    positions = jnp.arange(NEW, dtype=jnp.int32)
    live = (positions[None, :] < seq_lengths[:, None]).astype(jnp.float32)
    carried, readings = run_delta(
        delta_state, query_unit, key_unit, value_act, write_rate, log_keep, live
    )
    normed = readings * lax.rsqrt(jnp.mean(readings * readings, axis=-1, keepdims=True) + EPS)
    normed = normed * head_gain * jax.nn.silu(outgate)
    mixed = normed.reshape(own_rows, heads_here * head_size).astype(jnp.bfloat16)
    out_terms = jnp.dot(gather_directly(mixed, KV, 0), w_out, preferred_element_type=jnp.float32)
    attended = sent_and_summed(out_terms.astype(jnp.bfloat16), "tp", 0)
    hidden_state = (layer_input.astype(jnp.float32) + attended).astype(jnp.bfloat16)
    hidden_rows = gather_directly(hidden_state, "tp", 0)
    hidden_wide = hidden_rows.astype(jnp.float32)
    mixer_squares = jnp.sum(hidden_wide * hidden_wide, axis=1)
    mixer_part = lax.dynamic_slice_in_dim(mixer_gain, feature_anchor, feature_part).astype(
        jnp.float32
    )
    normed_mid = (hidden_wide * mixer_part).astype(jnp.bfloat16)
    gate_terms = jnp.dot(normed_mid, w_gate, preferred_element_type=jnp.float32)
    up_terms = jnp.dot(normed_mid, w_up, preferred_element_type=jnp.float32)
    gate_rows, up_rows, square_rows = (
        scatter_axes(gate_terms.astype(jnp.bfloat16), KV, 0).astype(jnp.float32),
        scatter_axes(up_terms.astype(jnp.bfloat16), KV, 0).astype(jnp.float32),
        scatter_axes(mixer_squares.astype(jnp.bfloat16), KV, 0).astype(jnp.float32),
    )
    mixer_scale = lax.rsqrt(square_rows / D + EPS)[:, None]
    activated = (jax.nn.silu(mixer_scale * gate_rows) * (mixer_scale * up_rows)).astype(
        jnp.bfloat16
    )
    mixer_terms = jnp.dot(whole_of(activated, KV, 0), w_down, preferred_element_type=jnp.float32)
    mixer_out = sent_and_summed(mixer_terms.astype(jnp.bfloat16), "tp", 0)
    layer_output = (hidden_state.astype(jnp.float32) + mixer_out).astype(jnp.bfloat16)
    return (layer_output, carried)


def solution(mesh):
    split = Mesh(mesh.devices.reshape(8, 4, mesh.shape["tp"]), ("kv_0", "kv_1", "tp"))
    in_specs = (
        P("tp", KV),
        P(KV),
        P(KV, "tp", None, None),
        P(),
        P(KV, "tp"),
        P(KV, "tp"),
        P(KV, "tp"),
        P(KV, "tp"),
        P(KV, "tp"),
        P(KV, "tp"),
        P("tp"),
        P(),
        P("tp", KV),
        P(),
        P(KV, "tp"),
        P(KV, "tp"),
        P("tp", KV),
    )
    out_specs = (P("tp", KV), P(KV, "tp", None, None))
    return jax.shard_map(local, mesh=split, in_specs=in_specs, out_specs=out_specs, check_vma=False)
```

profile of v0, /device:TPU:1, one launch (start us, length us, event | category | flops | bytes accessed | tf_op | source)
XLA Modules:
  0.0 537.7 jit_solution(10326635887785370400)
XLA Ops:
  7.2 1.5 broadcast_in_dim.6
  8.8 6.5 %all-to-all-start = ((bf16[8,128,128]{2,1,0:T(8,128)(2,1)}), bf16[8,128,128]{2,1,0:T(8,128)(2,1)S(1)}, u32[]{:S(2)}, u32[]{:S(2)}) async-start(bf16[8,128,128]{2,1,0:T(8,128)(2,1)} %broadcast_in_dim.6), calls=%async_computation | async-start | bytes 524288 | tf_op jit(solution)/shard_map/all_to_all | solution.py:23
  15.3 0.8 dynamic-slice_convert_fusion.2
  16.0 5.7 %all-to-all-done = bf16[8,128,128]{2,1,0:T(8,128)(2,1)S(1)} async-done(((bf16[8,128,128]{2,1,0:T(8,128)(2,1)}), bf16[8,128,128]{2,1,0:T(8,128)(2,1)S(1)}, u32[]{:S(2)}, u32[]{:S(2)}) %all-to-all-start) | async-done | bytes 262176 | tf_op jit(solution)/shard_map/all_to_all | solution.py:23
  22.1 1.2 convolution_convert_fusion.2
  23.3 1.2 convolution_convert_fusion.3
  24.4 1.1 convolution_convert_fusion.4
  25.6 1.1 convolution_convert_fusion.5
  26.9 4.2 concatenate.7
  31.1 2.6 copy.207
  33.8 216.1 %reduce-scatter.16.cloned.1.call-done = bf16[32,1029]{1,0:T(8,128)(2,1)} async-done(((bf16[1024,1029]{1,0:T(8,128)(2,1)}), bf16[32,1029]{1,0:T(8,128)(2,1)}) %reduce-scatter.16.cloned.1.call-update) | async-done | bytes 65872 | tf_op jit(solution)/shard_map/reduce_scatter | solution.py:33
  249.9 0.7 slice.143
  250.7 0.8 add_rsqrt_fusion
  252.2 0.8 convert_multiply_fusion.2
  254.3 1.0 fusion.47
  255.4 1.1 fusion
  256.6 1.4 fusion.41
  258.2 1.9 fusion.2
  260.2 1.9 fusion.3
  262.2 1.4 fusion.43
  263.7 1.1 fusion.1
  264.9 1.5 multiply_add_fusion
  266.4 1.0 fusion.37
  267.7 0.8 fusion.19
  268.6 19.2 %all_to_all.25 = bf16[32,32,256]{2,1,0:T(8,128)(2,1)S(1)} all-to-all(bf16[32,32,256]{2,1,0:T(8,128)(2,1)S(1)} %broadcast_in_dim.7), channel_id=1, replica_groups=mesh['kv_0'=8,'kv_1'=4,'tp'=8] {'kv_0','kv_1'}, dimensions={0} | all-to-all | bytes 1048576 | tf_op jit(solution)/shard_map/all_to_all | solution.py:23
  287.8 0.3 convolution_convert_fusion.7
  288.1 17.8 %all_to_all.26 = bf16[8,128,128]{2,1,0:T(8,128)(2,1)S(1)} all-to-all(bf16[8,128,128]{2,1,0:T(8,128)(2,1)S(1)} %bitcast.150), channel_id=1, replica_groups=mesh['kv_0'=8,'kv_1'=4,'tp'=8] {'tp'}, dimensions={0} | all-to-all | bytes 524288 | tf_op jit(solution)/shard_map/all_to_all | solution.py:48
  305.9 0.7 broadcast_in_dim.8
  306.6 4.4 all-to-all-start.3
  311.0 0.8 dynamic-slice_convert_fusion.1
  311.7 5.7 %all-to-all-done.3 = bf16[8,128,128]{2,1,0:T(8,128)(2,1)S(1)} async-done(((bf16[8,128,128]{2,1,0:T(8,128)(2,1)}), bf16[8,128,128]{2,1,0:T(8,128)(2,1)S(1)}, u32[]{:S(2)}, u32[]{:S(2)}) %all-to-all-start.3) | async-done | bytes 262176 | tf_op jit(solution)/shard_map/all_to_all | solution.py:23
  317.6 2.5 convolution_convert_fusion
  320.2 2.5 convolution_convert_fusion.1
  322.7 33.6 %reduce-scatter.12.cloned.1.call-done = bf16[128,1408]{1,0:T(8,128)(2,1)} async-done(((bf16[1024,1408]{1,0:T(8,128)(2,1)}), bf16[128,1408]{1,0:T(8,128)(2,1)}) %reduce-scatter.12.cloned.1.call-update) | async-done | bytes 360464 | tf_op jit(solution)/shard_map/reduce_scatter | solution.py:55
  356.4 46.7 %reduce-scatter.8.cloned.1.call-done = bf16[128,1408]{1,0:T(8,128)(2,1)} async-done(((bf16[1024,1408]{1,0:T(8,128)(2,1)}), bf16[128,1408]{1,0:T(8,128)(2,1)}) %reduce-scatter.8.cloned.1.call-update) | async-done | bytes 360464 | tf_op jit(solution)/shard_map/reduce_scatter | solution.py:55
  403.2 0.7 dynamic-slice.2
  403.9 0.6 dynamic-slice
  405.7 0.2 multiply_reduce_fusion
  405.9 13.1 %all-reduce = bf16[1024]{0:T(1024)(128)(2,1)S(1)} all-reduce(bf16[1024]{0:T(1024)(128)(2,1)S(1)} %bitcast.158), channel_id=3, replica_groups=mesh['kv_0'=8,'kv_1'=4,'tp'=8] {'kv_0'}, use_global_device_ids=true, to_apply=%region_7.8.clone | all-reduce | flops 1024 | bytes 4096
  419.1 8.2 %all-reduce.1 = bf16[128]{0:T(256)(128)(2,1)S(1)} all-reduce(bf16[128]{0:T(256)(128)(2,1)S(1)} %dynamic-slice.1), channel_id=4, replica_groups=mesh['kv_0'=8,'kv_1'=4,'tp'=8] {'kv_1'}, use_global_device_ids=true, to_apply=%region_8.9.clone | all-reduce | flops 128 | bytes 512
  427.4 3.4 reduce-scatter.14.cloned.1.call-done
  430.7 25.7 %reduce-scatter.10.cloned.1.call-done = bf16[32,1408]{1,0:T(8,128)(2,1)} async-done(((bf16[128,1408]{1,0:T(8,128)(2,1)}), bf16[32,1408]{1,0:T(8,128)(2,1)}) %reduce-scatter.10.cloned.1.call-update) | async-done | bytes 90128 | tf_op jit(solution)/shard_map/reduce_scatter | solution.py:55
  456.4 1.1 multiply_convert_fusion
  457.5 11.5 %all_gather.6 = bf16[128,1408]{1,0:T(8,128)(2,1)} all-gather(bf16[32,1408]{1,0:T(8,128)(2,1)S(1)} %multiply_convert_fusion), channel_id=1, replica_groups=mesh['kv_0'=8,'kv_1'=4,'tp'=8] {'kv_1'}, dimensions={0}, use_global_device_ids=true | all-gather | bytes 450560 | tf_op jit(solution)/shard_map/all_gather | solution.py:62
  469.0 45.4 %all-gather.2.cloned.1.call-done = bf16[1024,1408]{1,0:T(8,128)(2,1)} async-done(((bf16[128,1408]{1,0:T(8,128)(2,1)}), bf16[1024,1408]{1,0:T(8,128)(2,1)}) %all-gather.2.cloned.1.call-update) | async-done | bytes 2883600 | tf_op jit(solution)/shard_map/all_gather | solution.py:62
  514.4 2.7 convolution_convert_fusion.6
  517.1 13.1 %all_to_all.27 = bf16[8,128,128]{2,1,0:T(8,128)(2,1)S(1)} all-to-all(bf16[8,128,128]{2,1,0:T(8,128)(2,1)S(1)} %bitcast.151), channel_id=1, replica_groups=mesh['kv_0'=8,'kv_1'=4,'tp'=8] {'tp'}, dimensions={0} | all-to-all | bytes 524288 | tf_op jit(solution)/shard_map/all_to_all | solution.py:48
  530.3 0.6 add_convert_fusion
  (115 shorter events, 4.0 us)
Async XLA Ops:
  7.2 310.4 %copy-start = (bf16[128,1408]{1,0:T(8,128)(2,1)S(1)}, bf16[128,1408]{1,0:T(8,128)(2,1)}, u32[]{:S(2)}) copy-start(bf16[128,1408]{1,0:T(8,128)(2,1)} %param.32) | copy-start | bytes 1081348
  7.2 17.3 %copy-start.5 = (bf16[128,256]{1,0:T(8,128)(2,1)S(1)}, bf16[128,256]{1,0:T(8,128)(2,1)}, u32[]{:S(2)}) copy-start(bf16[128,256]{1,0:T(8,128)(2,1)} %param.22) | copy-start | bytes 196612
  7.2 18.4 %copy-start.6 = (bf16[128,256]{1,0:T(8,128)(2,1)S(1)}, bf16[128,256]{1,0:T(8,128)(2,1)}, u32[]{:S(2)}) copy-start(bf16[128,256]{1,0:T(8,128)(2,1)} %param.21) | copy-start | bytes 196612
  7.2 19.5 %copy-start.8 = (bf16[128,2]{0,1:T(2,128)(2,1)S(1)}, bf16[128,2]{0,1:T(2,128)(2,1)}, u32[]{:S(2)}) copy-start(bf16[128,2]{0,1:T(2,128)(2,1)} %param.26) | copy-start | bytes 1540
  7.2 19.5 %copy-start.9 = (bf16[128,2]{0,1:T(2,128)(2,1)S(1)}, bf16[128,2]{0,1:T(2,128)(2,1)}, u32[]{:S(2)}) copy-start(bf16[128,2]{0,1:T(2,128)(2,1)} %param.25) | copy-start | bytes 1540
  8.8 13.0 %all-to-all-start = ((bf16[8,128,128]{2,1,0:T(8,128)(2,1)}), bf16[8,128,128]{2,1,0:T(8,128)(2,1)S(1)}, u32[]{:S(2)}, u32[]{:S(2)}) async-start(bf16[8,128,128]{2,1,0:T(8,128)(2,1)} %broadcast_in_dim.6), calls=%async_computation | async-start | bytes 524288 | tf_op jit(solution)/shard_map/all_to_all | solution.py:23
  15.3 234.6 %reduce-scatter.16.cloned.1.call-start = ((), (), s32[]{:S(2)}) async-start(), calls=%async_computation.15 | async-start | bytes 2433024 | tf_op jit(solution)/shard_map/reduce_scatter | solution.py:33
  31.1 2.7 copy-start.12
  31.1 2.7 copy-start.13
  31.1 2.7 copy-start.10
  33.7 220.6 %copy-start.1 = (f32[8,2,128,128]{3,2,1,0:T(8,128)S(1)}, f32[8,2,128,128]{3,2,1,0:T(8,128)}, u32[]{:S(2)}) copy-start(f32[8,2,128,128]{3,2,1,0:T(8,128)} %param.19) | copy-start | bytes 3145732
  263.7 24.1 %copy-start.7 = (bf16[256,128]{1,0:T(8,128)(2,1)S(1)}, bf16[256,128]{1,0:T(8,128)(2,1)}, u32[]{:S(2)}) copy-start(bf16[256,128]{1,0:T(8,128)(2,1)} %param.29) | copy-start | bytes 196612
  264.9 41.0 %copy-start.4 = (bf16[128,128]{1,0:T(8,128)(2,1)S(1)}, bf16[128,128]{1,0:T(8,128)(2,1)}, u32[]{:S(2)}) copy-start(bf16[128,128]{1,0:T(8,128)(2,1)} %param.17) | copy-start | bytes 98308
  266.4 51.1 %copy-start.2 = (f32[8,2,128,128]{3,2,1,0:T(8,128)}, f32[8,2,128,128]{3,2,1,0:T(8,128)S(1)}, u32[]{:S(2)}) copy-start(f32[8,2,128,128]{3,2,1,0:T(8,128)S(1)} %multiply_add_fusion) | copy-start | bytes 3145732
  306.6 10.8 %all-to-all-start.3 = ((bf16[8,128,128]{2,1,0:T(8,128)(2,1)}), bf16[8,128,128]{2,1,0:T(8,128)(2,1)S(1)}, u32[]{:S(2)}, u32[]{:S(2)}) async-start(bf16[8,128,128]{2,1,0:T(8,128)(2,1)} %broadcast_in_dim.8), calls=%async_computation.3 | async-start | bytes 524288 | tf_op jit(solution)/shard_map/all_to_all | solution.py:23
  311.0 45.4 %reduce-scatter.12.cloned.1.call-start = ((), (), s32[]{:S(2)}) async-start(), calls=%async_computation.12 | async-start | bytes 3244032 | tf_op jit(solution)/shard_map/reduce_scatter | solution.py:55
  317.6 2.6 copy-start.3
  320.1 83.1 %copy-start.15 = (u32[256]{0:T(256)S(1)}, u32[256]{0:T(256)}, u32[]{:S(2)}) copy-start(u32[256]{0:T(256)} %constant.54) | copy-start | bytes 3076
  320.1 83.8 %copy-start.14 = (u32[256]{0:T(256)S(1)}, u32[256]{0:T(256)}, u32[]{:S(2)}) copy-start(u32[256]{0:T(256)} %constant.50) | copy-start | bytes 3076
  320.1 83.0 %reduce-scatter.8.cloned.1.call-start = ((), (), s32[]{:S(2)}) async-start(), calls=%async_computation.10 | async-start | bytes 3244032 | tf_op jit(solution)/shard_map/reduce_scatter | solution.py:55
  322.7 191.7 %copy-start.11 = (bf16[1408,128]{1,0:T(8,128)(2,1)S(1)}, bf16[1408,128]{1,0:T(8,128)(2,1)}, u32[]{:S(2)}) copy-start(bf16[1408,128]{1,0:T(8,128)(2,1)} %param.33) | copy-start | bytes 1081348
  322.7 108.0 %reduce-scatter.14.cloned.1.call-start = ((), (), s32[]{:S(2)}) async-start(), calls=%async_computation.13 | async-start | bytes 450560 | tf_op jit(solution)/shard_map/reduce_scatter | solution.py:55
  356.4 100.1 %reduce-scatter.10.cloned.1.call-start = ((), (), s32[]{:S(2)}) async-start(), calls=%async_computation.11 | async-start | bytes 450560 | tf_op jit(solution)/shard_map/reduce_scatter | solution.py:55
  403.1 111.2 %all-gather.2.cloned.1.call-start = ((), (), s32[]{:S(2)}) async-start(), calls=%async_computation.14 | async-start | bytes 3244032 | tf_op jit(solution)/shard_map/all_gather | solution.py:62
Sparse Core Ops, SparseCore 0:
  33.9 215.9 reduce-scatter.15
  320.2 36.1 reduce-scatter.11
  358.9 44.1 reduce-scatter.7
  405.5 25.1 reduce-scatter.13
  433.1 23.2 reduce-scatter.9
  469.1 45.2 all-gather.1
where the time goes:
time: 539 us; the launch traced here: 538 us
  waiting for transfers between devices  382 us (71%)
  blocking collectives  82.8 us (15%)
  matrix products  23.8 us (4%)
  between operations  15.9 us (3%)
  local copies, waits for them, and re-layouts  12.6 us (2%)
  starting transfers between devices  11 us (2%)
  other arithmetic  9.28 us (2%)
    reduce_scatter x1, waiting for transfers between devices, sent_together(): lax.psum_scatter(both, axis, scatter_dimension=dim, tiled=True)  216 us
    reduce_scatter x4, waiting for transfers between devices, scatter_axes(): nearer = lax.psum_scatter(array, axes[0], scatter_dimension=dim, tiled=True)  109 us
    all_gather x1, waiting for transfers between devices, whole_of(): filled = lax.all_gather(filled, axes[number], axis=dim, tiled=True)  45.4 us
    all_to_all x2, blocking collectives, sent_and_summed(): lax.all_to_all(cut_along(array, dim, length), axis, 0, 0, tiled=True)  30.9 us
    unnamed x2, blocking collectives  21.3 us
    all_to_all x1, blocking collectives, from_everyone(): return lax.all_to_all(copies, axis, split_axis=0, concat_axis=0, tiled=True)  19.2 us
    all_to_all x2, waiting for transfers between devices, from_everyone(): return lax.all_to_all(copies, axis, split_axis=0, concat_axis=0, tiled=True)  11.5 us
    all_gather x1, blocking collectives, whole_of(): filled = lax.all_gather(filled, axes[number], axis=dim, tiled=True)  11.5 us
  transfers between devices with their start and end apart: 8, of which 8 were waited for; matrix products, arithmetic and copies ran while one was open for 1% of the time, Pallas kernels for 0%

commit v1 on v0

v1 whole, which is shorter than its diff:
```python
import functools

import jax
import jax.numpy as jnp
from jax import lax
from jax.experimental import pallas as pl
from jax.experimental.pallas import tpu as pltpu
from jax.sharding import Mesh
from jax.sharding import PartitionSpec as P

D = 4096
NEW = 4
EPS = 1e-06
NZ, NX, NY, NC = 8, 4, 4, 2
NTP = NY * NC
R = 128
F = 128
WIN = 384
MESH = pl.DeviceIdType.MESH
BF = jnp.bfloat16
F32 = jnp.float32
PLANE = [(dx, dy) for dx in range(NX) for dy in range(NY) if dx or dy]
NSEM = 224


def silu(a):
    return a * jax.nn.sigmoid(a)


def rows_of(k):
    return pl.ds(pl.multiple_of(k * R, R), R)


def dot_t(a, b):
    return lax.dot_general(a, b, (((1,), (1,)), ((), ())), preferred_element_type=F32)


class Links:
    def __init__(self, send, recv):
        self.send, self.recv, self.n, self.all = send, recv, 0, []
        self.z, self.x = lax.axis_index("z"), lax.axis_index("x")
        self.y, self.c = lax.axis_index("y"), lax.axis_index("c")

    def copy(self, src, dst, dz=0, dx=0, dy=0, dc=0):
        to = (
            lax.rem(self.z + dz, NZ),
            lax.rem(self.x + dx, NX),
            lax.rem(self.y + dy, NY),
            lax.rem(self.c + dc, NC),
        )
        return self.copy_to(src, dst, to)

    def copy_to(self, src, dst, to):
        made = pltpu.make_async_remote_copy(
            src_ref=src,
            dst_ref=dst,
            send_sem=self.send.at[self.n],
            recv_sem=self.recv.at[self.n],
            device_id=to,
            device_id_type=MESH,
        )
        self.n += 1
        self.all.append(made)
        made.start()
        return made

    def drain(self):
        for made in self.all:
            made.wait_send()


def enter(links):
    z, x, y, c = links.z, links.x, links.y, links.c
    barrier = pltpu.get_barrier_semaphore()
    to = [(dz, 0, 0, 0) for dz in range(1, NZ)]
    to += [(0, dx, dy, 0) for dx, dy in PLANE]
    to += [(0, 0, dy, 1) for dy in range(NY)]
    for dz, dx, dy, dc in to:
        pl.semaphore_signal(
            barrier,
            inc=1,
            device_id=(lax.rem(z + dz, NZ), lax.rem(x + dx, NX), lax.rem(y + dy, NY), lax.rem(c + dc, NC)),
            device_id_type=MESH,
        )
    pl.semaphore_wait(barrier, len(to))


def plane_gather_start(links, src, buf):
    tp = links.y * NC + links.c
    here = buf.at[links.x, rows_of(tp)]
    straight = [links.copy(src, here, dx=dx, dy=dy) for dx, dy in PLANE]
    forward = [links.copy(src, here, dc=1)]
    return straight, forward


def plane_gather_finish(links, buf, straight, forward):
    for (dx, dy), made in zip(PLANE, straight):
        made.wait_recv()
        xs, ys = lax.rem(links.x - dx + NX, NX), lax.rem(links.y - dy + NY, NY)
        block = buf.at[xs, rows_of(ys * NC + links.c)]
        forward.append(links.copy(block, block, dc=1))
    for made in forward:
        made.wait_recv()


def ring_sum(links, block, sendbuf, recvbuf, width):
    half = width // 2
    made = {}

    def send(way, step, side):
        offset = 4 - step if way == 0 else 4 + step
        lanes = pl.ds(side * half, half)
        value = block(offset)[:, side * half : (side + 1) * half]
        before = made.get((way, step - 1, side))
        if before is not None:
            before.wait_recv()
            value = value + recvbuf[way, step - 1, side].astype(F32)
        sendbuf[way, step, side] = value.astype(BF)
        made[way, step, side] = links.copy(
            sendbuf.at[way, step, side], recvbuf.at[way, step, side], dz=1 if way == 0 else NZ - 1
        )

    for way, step, side in [(0, 0, 0), (1, 0, 1), (0, 1, 1), (1, 1, 0), (0, 1, 0), (1, 1, 1)]:
        send(way, step, side)
    for step in (2, 3):
        for side in (1, 0):
            send(0, step, side)
            send(1, step, 1 - side)
    own = block(0)
    total = []
    for side in (0, 1):
        for way in (0, 1):
            made[way, 3, side].wait_recv()
        total.append(
            own[:, side * half : (side + 1) * half]
            + recvbuf[0, 3, side].astype(F32)
            + recvbuf[1, 3, side].astype(F32)
        )
    return jnp.concatenate(total, axis=1)


def normalize(buf, gain, out, stats, rates):
    sub = lax.broadcasted_iota(jnp.int32, (8, R), 0)
    ones = jnp.ones((16, F), BF)

    def one(b, _):
        at = rows_of(b)
        squares = jnp.zeros((R, F), F32)
        for k in range(NX):
            wide = buf[k, at, :].astype(F32)
            squares = squares + wide * wide
            out[at, k * F : (k + 1) * F] = (wide * gain[:, k * F : (k + 1) * F]).astype(BF)
        high = squares.astype(BF)
        low = (squares - high.astype(F32)).astype(BF)
        row = (dot_t(ones, high) + dot_t(ones, low))[:8]
        stat = jnp.where(sub == 4, row, 0.0)
        if rates is not None:
            for k in range(NX):
                stat = stat + dot_t(rates[k], out[at, k * F : (k + 1) * F])[:8]
        stats[b] = stat
        return 0

    lax.fori_loop(0, NTP, one, 0)


def stats_exchange(links, stats, got):
    made = []
    for dz in range(1, NZ):
        made.append(links.copy(stats.at[lax.rem(links.z + dz, NZ)], got.at[dz], dz=dz))
    return made


def stats_total(links, stats, got, made):
    total = stats[links.z]
    for dz, one in enumerate(made, 1):
        one.wait_recv()
        total = total + got[dz]
    wide = jnp.concatenate([total, jnp.zeros((R - 8, R), F32)], axis=0)
    return wide.T


def body(
    x_ref, len_ref, state_ref, gain1_ref, wq, wk, wv, wo, rate_w_ref, rate_ref, head_gain_ref, w_out_ref, gain2_ref,
    w_gate, w_up, w_down,
    out_ref, next_ref,
    xbuf, nbuf, w4, wr, rw, p1, s1, r1, stats1, got1, pre, mine, cols, readings, mixed_own, mbuf, obuf, orecv,
    hown, hbuf, stats2, got2, wg, wu, wd, p2, s2, r2, act_own, abuf, part, psend, precv, fsend, frecv,
    local, send, recv,
):
    links = Links(send, recv)
    z, x, y, c = links.z, links.x, links.y, links.c
    tp = y * NC + c
    kv = z * NX + x

    locals_ = [pltpu.make_async_copy(w, w4.at[i], local.at[i]) for i, w in enumerate((wq, wk, wv, wo))]

    def window(at):
        return pl.ds(pl.multiple_of((at * 3 - at // (NX - 1)) * F, F), WIN)

    feats = pl.ds(pl.multiple_of(x * F, F), F)
    own_copies = [
        pltpu.make_async_copy(x_ref, xbuf.at[x, rows_of(tp)], local.at[4]),
        pltpu.make_async_copy(rate_w_ref, rw.at[x], local.at[5]),
        pltpu.make_async_copy(w_gate.at[:, window(x)], wg.at[feats], local.at[6]),
        pltpu.make_async_copy(w_up.at[:, window(x)], wu.at[feats], local.at[7]),
        pltpu.make_async_copy(w_down.at[window(x)], wd.at[x], local.at[8]),
    ]
    for one in locals_ + own_copies:
        one.start()
    enter(links)

    straight, forward = plane_gather_start(links, x_ref, xbuf)
    for one in locals_:
        one.wait()
    own_w = pltpu.make_async_copy(w4.at[x], wr.at[feats], local.at[9])
    own_w.start()
    early, late = [], []
    for dx in range(1, NX):
        to = lax.rem(x + dx, NX)
        early.append(links.copy(w4.at[to], wr.at[feats], dx=dx))
        early.append(links.copy(rate_w_ref, rw.at[x], dx=dx))
    for dx in range(1, NX):
        to = lax.rem(x + dx, NX)
        late.append(links.copy(w_gate.at[:, window(to)], wg.at[feats], dx=dx))
        late.append(links.copy(w_up.at[:, window(to)], wu.at[feats], dx=dx))
    for dx in range(1, NX):
        to = lax.rem(x + dx, NX)
        late.append(links.copy(w_down.at[window(to)], wd.at[x], dx=dx))
    for one in own_copies[:2] + [own_w]:
        one.wait()
    plane_gather_finish(links, xbuf, straight, forward)
    for one in early:
        one.wait_recv()

    eighth = lax.broadcasted_iota(jnp.int32, (8, NX * F), 0) == z
    gain1 = jnp.sum(jnp.where(eighth, gain1_ref[...].astype(F32), 0.0), axis=0, keepdims=True)
    gain2 = jnp.sum(jnp.where(eighth, gain2_ref[...].astype(F32), 0.0), axis=0, keepdims=True)
    normalize(xbuf, gain1, nbuf, stats1, rw)
    made = stats_exchange(links, stats1, got1)

    ready = set()

    def projected(offset):
        if offset not in ready:
            ready.add(offset)
            p1[offset] = jnp.dot(
                nbuf[rows_of(lax.rem(z + offset, NZ)), :], wr[...], preferred_element_type=F32
            )
        return p1[offset]

    mine[...] = ring_sum(links, projected, s1, r1, 256).astype(BF)
    quarter = pl.ds(pl.multiple_of(x * 32, 32), 32)
    own_pre = pltpu.make_async_copy(mine.at[quarter], pre.at[x], local.at[10])
    own_pre.start()
    parts = []
    for dx in range(1, NX):
        to = lax.rem(x + dx, NX)
        parts.append(links.copy(mine.at[pl.ds(pl.multiple_of(to * 32, 32), 32)], pre.at[x], dx=dx))
    cols[...] = stats_total(links, stats1, got1, made)
    stat = cols[quarter, :]
    scale = lax.rsqrt(stat[:, 4:5] / D + EPS)
    lane = lax.broadcasted_iota(jnp.int32, (32, R), 1)
    row = lax.broadcasted_iota(jnp.int32, (32, R), 0)
    live = jnp.zeros((32, R), F32)
    for s in range(8):
        inside = (row // NEW == s) & (lax.rem(row, NEW) < len_ref[s])
        live = live + jnp.where(inside, 1.0, 0.0)
    rated = stat * scale
    beta = jax.nn.sigmoid(rated) * live
    rate = jnp.where(lane == 2, rate_ref[0], jnp.where(lane == 3, rate_ref[1], 0.0))
    softplus = jnp.maximum(rated, 0.0) + jnp.log1p(jnp.exp(-jnp.abs(rated)))
    keep = jnp.exp(-rate * softplus * live)
    own_pre.wait()
    for one in parts:
        one.wait_recv()
    query, key, value = (silu(pre[i].astype(F32) * scale) for i in range(3))
    gate = silu(pre[3].astype(F32) * scale)

    def unit(a):
        return a * lax.rsqrt(jnp.sum(a * a, axis=1, keepdims=True) + EPS)

    stacked = []
    for h in range(2):
        at = slice(h * F, (h + 1) * F)
        stacked += [unit(query[:, at]) * F ** (-0.5), unit(key[:, at])]
    turned = jnp.concatenate(stacked, axis=0).T
    for s in range(8):
        for h in range(2):
            state = state_ref[s, h]
            for t in range(NEW):
                r = s * NEW + t
                q_col = turned[:, h * 64 + r : h * 64 + r + 1]
                k_col = turned[:, h * 64 + 32 + r : h * 64 + 33 + r]
                hold = keep[r : r + 1, 2 + h : 3 + h]
                recalled = jnp.sum(k_col * state, axis=0, keepdims=True)
                update = beta[r : r + 1, h : h + 1] * (value[r : r + 1, h * F : (h + 1) * F] - hold * recalled)
                state = hold * state + k_col * update
                readings[r : r + 1, h * F : (h + 1) * F] = jnp.sum(q_col * state, axis=0, keepdims=True)
            next_ref[s, h] = state
    for h in range(2):
        at = slice(h * F, (h + 1) * F)
        read = readings[:, at] * live
        normed = read * lax.rsqrt(jnp.mean(read * read, axis=1, keepdims=True) + EPS)
        mixed_own[:, at] = (normed * head_gain_ref[...] * gate[:, at]).astype(BF)

    def slot(at):
        return mbuf.at[x, pl.ds(pl.multiple_of(at * 32, 32), 32)]

    own_mixed = pltpu.make_async_copy(mixed_own, slot(z), local.at[11])
    own_mixed.start()
    along_z = [links.copy(mixed_own, slot(z), dz=dz) for dz in range(1, NZ)]
    along_x = [links.copy(mixed_own, slot(z), dx=dx) for dx in range(1, NX)]
    for dz in (1, 7, 2, 6, 3, 5, 4):
        along_z[dz - 1].wait_recv()
        block = slot(lax.rem(z - dz + NZ, NZ))
        along_x += [links.copy(block, block, dx=dx) for dx in range(1, NX)]
    own_mixed.wait()
    for one in along_x:
        one.wait_recv()
    for k in range(NX):
        terms = jnp.dot(mbuf[k], w_out_ref[...], preferred_element_type=F32).astype(BF)
        for b in range(NTP):
            obuf[b, k * 32 : (k + 1) * 32, :] = terms[b * 32 : (b + 1) * 32]
    made = []
    for k in range(1, NTP):
        to = lax.rem(tp + k, NTP)
        made.append(links.copy_to(obuf.at[to], orecv.at[k], (z, x, to // NC, lax.rem(to, NC))))
    attended = obuf[tp].astype(F32)
    for k, one in enumerate(made, 1):
        one.wait_recv()
        attended = attended + orecv[k].astype(F32)
    hidden = (x_ref[...].astype(F32) + attended).astype(BF)
    hown[...] = hidden

    own_hidden = pltpu.make_async_copy(hown, hbuf.at[x, rows_of(tp)], local.at[12])
    own_hidden.start()
    straight, forward = plane_gather_start(links, hown, hbuf)
    own_hidden.wait()
    plane_gather_finish(links, hbuf, straight, forward)
    normalize(hbuf, gain2, nbuf, stats2, None)
    made = stats_exchange(links, stats2, got2)
    for one in own_copies[2:]:
        one.wait()
    for one in late:
        one.wait_recv()

    ready2 = set()

    def mixer(offset):
        if offset not in ready2:
            ready2.add(offset)
            rows = nbuf[rows_of(lax.rem(z + offset, NZ)), :]
            p2[offset, :, :WIN] = jnp.dot(rows, wg[...], preferred_element_type=F32)
            p2[offset, :, WIN:] = jnp.dot(rows, wu[...], preferred_element_type=F32)
        return p2[offset]

    total = ring_sum(links, mixer, s2, r2, 2 * WIN)
    scale2 = lax.rsqrt(stats_total(links, stats2, got2, made)[:, 4:5] / D + EPS)
    activated = silu(scale2 * total[:, :WIN]) * (scale2 * total[:, WIN:])
    again = (lax.broadcasted_iota(jnp.int32, (R, WIN), 1) < F) & (x == NX - 1)
    act_own[...] = jnp.where(again, 0.0, activated).astype(BF)

    def piece(at, side):
        return abuf.at[at, pl.ds(side * 64, 64)]

    own_act = pltpu.make_async_copy(act_own, abuf.at[z], local.at[13])
    own_act.start()
    going = {}
    for side in (0, 1):
        for way in (0, 1):
            going[way, 0, side] = links.copy(
                act_own.at[pl.ds(side * 64, 64)], piece(z, side), dz=1 if way == 0 else NZ - 1
            )
    for step in (1, 2, 3):
        for side in (0, 1):
            for way in (0, 1):
                if step == 3 and side != way:
                    continue
                going[way, step - 1, side].wait_recv()
                block = piece(lax.rem(z + (NZ - step if way == 0 else step), NZ), side)
                going[way, step, side] = links.copy(block, block, dz=1 if way == 0 else NZ - 1)
    own_act.wait()
    for one in ((0, 2, 1), (1, 2, 0), (0, 3, 0), (1, 3, 1)):
        going[one].wait_recv()
    for b in range(NZ):
        for k in range(NX):
            part[b, :, k * F : (k + 1) * F] = jnp.dot(abuf[b], wd[k], preferred_element_type=F32)
    over = []
    for k in range(NY):
        psend[k] = part[k * NC + 1 - c].astype(BF)
        over.append(links.copy(psend.at[k], precv.at[k], dc=1))
    for k in range(NY):
        over[k].wait_recv()
        both = (part[k * NC + c] + precv[k].astype(F32)).astype(BF)
        for j in range(NX):
            fsend[k, j] = both[:, j * F : (j + 1) * F]
    last = []
    for i, (dx, dy) in enumerate(PLANE):
        last.append(
            links.copy(fsend.at[lax.rem(y + dy, NY), lax.rem(x + dx, NX)], frecv.at[i], dx=dx, dy=dy)
        )
    result = hown[...].astype(F32) + fsend[y, x].astype(F32)
    for i, one in enumerate(last):
        one.wait_recv()
        result = result + frecv[i].astype(F32)
    out_ref[...] = result.astype(BF)
    links.drain()
    assert links.n <= NSEM, links.n


def local(
    layer_input, seq_lengths, delta_state, attn_gain, w_query, w_key, w_value, w_outgate, w_write, w_forget,
    forget_rate, head_gain, w_out, mixer_gain, w_gate, w_up, w_down,
):
    rate_w = jnp.concatenate([w_write.T, w_forget.T, jnp.zeros((12, F), BF)], axis=0)
    vmem = pl.BlockSpec(memory_space=pltpu.VMEM)
    smem = pl.BlockSpec(memory_space=pltpu.SMEM)
    hbm = pl.BlockSpec(memory_space=pl.ANY)
    scratch = [
        ((NX, NTP * R, F), BF),
        ((NTP * R, NX * F), BF),
        ((4, F, 256), BF),
        ((NX * F, 256), BF),
        ((NX, 16, F), BF),
        ((NZ, R, 256), F32),
        ((2, 4, 2, R, 128), BF),
        ((2, 4, 2, R, 128), BF),
        ((NZ, 8, R), F32),
        ((NZ, 8, R), F32),
        ((NX, 32, 256), BF),
        ((R, 256), BF),
        ((R, R), F32),
        ((32, 256), F32),
        ((32, 256), BF),
        ((NX, NZ * 32, 256), BF),
        ((NTP, R, F), BF),
        ((NTP, R, F), BF),
        ((R, F), BF),
        ((NX, NTP * R, F), BF),
        ((NZ, 8, R), F32),
        ((NZ, 8, R), F32),
        ((NX * F, WIN), BF),
        ((NX * F, WIN), BF),
        ((NX, WIN, F), BF),
        ((NZ, R, 2 * WIN), F32),
        ((2, 4, 2, R, WIN), BF),
        ((2, 4, 2, R, WIN), BF),
        ((R, WIN), BF),
        ((NZ, R, WIN), BF),
        ((NZ, R, NX * F), F32),
        ((NY, R, NX * F), BF),
        ((NY, R, NX * F), BF),
        ((NY, NX, R, F), BF),
        ((NX * NY, R, F), BF),
    ]
    return pl.pallas_call(
        body,
        out_shape=(
            jax.ShapeDtypeStruct((R, F), BF),
            jax.ShapeDtypeStruct(delta_state.shape, F32),
        ),
        in_specs=[
            vmem, smem, vmem, vmem, hbm, hbm, hbm, hbm, vmem, smem, vmem, vmem, vmem, hbm, hbm, hbm,
        ],
        out_specs=(vmem, vmem),
        scratch_shapes=[pltpu.VMEM(shape, dtype) for shape, dtype in scratch]
        + [
            pltpu.SemaphoreType.DMA((14,)),
            pltpu.SemaphoreType.DMA((NSEM,)),
            pltpu.SemaphoreType.DMA((NSEM,)),
        ],
        compiler_params=pltpu.CompilerParams(
            collective_id=0, has_side_effects=True, vmem_limit_bytes=56 * 1024 * 1024
        ),
    )(
        layer_input, seq_lengths, delta_state, attn_gain.reshape(8, NX * F), w_query, w_key, w_value, w_outgate,
        rate_w, forget_rate, head_gain.reshape(1, F), w_out, mixer_gain.reshape(8, NX * F), w_gate, w_up, w_down,
    )


def solution(mesh):
    split = Mesh(mesh.devices.reshape(NZ, NX, NY, NC), ("z", "x", "y", "c"))
    kv, tp = ("z", "x"), ("y", "c")
    in_specs = (
        P(tp, kv), P(kv), P(kv, tp, None, None), P(), P(kv, tp), P(kv, tp), P(kv, tp), P(kv, tp), P(kv, tp),
        P(kv, tp), P(tp), P(), P(tp, kv), P(), P(kv, tp), P(kv, tp), P(tp, kv),
    )
    out_specs = (P(tp, kv), P(kv, tp, None, None))
    return jax.shard_map(local, mesh=split, in_specs=in_specs, out_specs=out_specs, check_vma=False)
```

time: 539 us -> 131 us (0.24)
  waiting for transfers between devices: 382 us -> 0 us
  Pallas kernels: 0 us -> 124 us
  blocking collectives: 82.8 us -> 0 us
  matrix products: 23.8 us -> 0 us
  between operations: 15.9 us -> 0.67 us
  starting transfers between devices: 11 us -> 0 us
  other arithmetic: 9.28 us -> 0.67 us
  local copies, waits for them, and re-layouts: 12.6 us -> 5.65 us
    reduce_scatter x5 -> x0, waiting for transfers between devices: 325 us -> none  [the longest x1 216 us: sent_together(): lax.psum_scatter(both, axis, scatter_dimension=dim, tiled=True)]
    pallas_call x0 -> x1, Pallas kernels: none -> 124 us  [local(): pl.pallas_call(body, out_shape=(jax.ShapeDtypeStruct((R, F), BF), jax.Sha...]
    all_to_all x3 -> x0, blocking collectives: 50.1 us -> none  [the longest x2 30.9 us: sent_and_summed(): lax.all_to_all(cut_along(array, dim, length), axis, 0, 0, tiled=True)]
    all_gather x1 -> x0, waiting for transfers between devices: 45.4 us -> none  [whole_of(): filled = lax.all_gather(filled, axes[number], axis=dim, tiled=True)]
    dot_general x17 -> x0, matrix products: 23.8 us -> none  [the longest x4 5.49 us: run_delta(): jnp.einsum('shk,shkv->shv', query_unit[:, position], carried, precision=l...]
    unnamed x2 -> x0, blocking collectives: 21.3 us -> none
    all_to_all x2 -> x0, waiting for transfers between devices: 11.5 us -> none  [from_everyone(): return lax.all_to_all(copies, axis, split_axis=0, concat_axis=0, tiled=True)]
    all_gather x1 -> x0, blocking collectives: 11.5 us -> none  [whole_of(): filled = lax.all_gather(filled, axes[number], axis=dim, tiled=True)]
  transfers between devices with their start and end apart: 8 -> 0, of which waited for: 8 -> 0; matrix products, arithmetic and copies ran while one was open for 1% -> 0% of each run, Pallas kernels for 0% -> 0%
where the time goes in v1:
time: 131 us
  Pallas kernels  124 us (95%)
  local copies, waits for them, and re-layouts  5.65 us (4%)
    pallas_call x1, Pallas kernels, local(): pl.pallas_call(body, out_shape=(jax.ShapeDtypeStruct((R, F), BF), jax.Sha...  124 us
    unnamed x10, local copies, waits for them, and re-layouts  4.34 us

profile of v1, /device:TPU:1, one launch (start us, length us, event | category | flops | bytes accessed | tf_op | source)
XLA Modules:
  0.0 130.5 jit_solution(11565727510910141673)
XLA Ops:
  0.6 0.0 copy-start
  0.7 0.0 copy-start.2
  0.7 0.0 copy-start.3
  0.7 0.1 pad.2.clone
  0.8 0.6 copy-done.2
  1.3 0.0 copy-done.3
  1.3 0.7 maximum_maximum_fusion.rate_w_ref
  2.0 0.0 copy-done
  2.0 0.0 copy-start.1
  2.0 0.6 reshape.13.gain1_ref
  2.6 0.1 copy-done.1
  2.7 0.6 reshape.15.gain2_ref
  3.3 123.5 %shard_map.176 = (bf16[128,128]{1,0:T(8,128)(2,1)}, f32[8,2,128,128]{3,2,1,0:T(8,128)}) custom-call(bf16[128,128]{1,0:T(8,128)(2,1)} %x_ref.1, s32[8]{0:T(128)} %len_ref.1, f32[8,2,128,128]{3,2,1,0:T(8,128)} %state_ref.1, bf16[8,512]{1,0:T(8,128)(2,1)} %reshape.13.gain1_ref, bf16[128,256]{1,0:T(8,128)(2,1)} %wq.1, bf16[128,256]{1,0:T(8,128)(2,1)} %wk.1, ...), custom_call_target="tpu_custom_call" | custom-call | tf_op jit(solution)/shard_map/pallas_call | solution.py:456
  126.8 1.4 %copy.21 = bf16[128,128]{1,0:T(8,128)(2,1)} copy(bf16[128,128]{1,0:T(8,128)(2,1)} %get-tuple-element.4) | data formatting | bytes 65536
  128.2 2.3 %copy.22 = f32[8,2,128,128]{3,2,1,0:T(8,128)} copy(f32[8,2,128,128]{3,2,1,0:T(8,128)} %get-tuple-element.5) | data formatting | bytes 2097152
  (1 shorter events, 0.0 us)
Async XLA Ops:
  0.6 1.4 %copy-start = (bf16[4096]{0:T(1024)(128)(2,1)S(1)}, bf16[4096]{0:T(1024)(128)(2,1)}, u32[]{:S(2)}) copy-start(bf16[4096]{0:T(1024)(128)(2,1)} %param.20) | copy-start | bytes 24580
  0.7 0.7 copy-start.2
  0.7 0.7 copy-start.3
  2.0 0.7 copy-start.1

commit v2 on v1

v2 whole, which is shorter than its diff:
```python
import functools

import jax
import jax.numpy as jnp
from jax import lax
from jax.experimental import pallas as pl
from jax.experimental.pallas import tpu as pltpu
from jax.sharding import Mesh
from jax.sharding import PartitionSpec as P

D = 4096
NEW = 4
EPS = 1e-06
NZ, NX, NY, NC = 8, 4, 4, 2
NTP = NY * NC
R = 128
F = 128
WIN = 384
MESH = pl.DeviceIdType.MESH
BF = jnp.bfloat16
F32 = jnp.float32
PLANE = [(dx, dy) for dx in range(NX) for dy in range(NY) if dx or dy]
NSEM = 260
VMEM_LIMIT = 58 * 1024 * 1024


def silu(a):
    return a * jax.nn.sigmoid(a)


def rows_of(k):
    return pl.ds(pl.multiple_of(k * R, R), R)


def dot_t(a, b):
    return lax.dot_general(a, b, (((1,), (1,)), ((), ())), preferred_element_type=F32)


class Links:
    def __init__(self, send, recv):
        self.send, self.recv, self.n, self.all = send, recv, 0, []
        self.z, self.x = lax.axis_index("z"), lax.axis_index("x")
        self.y, self.c = lax.axis_index("y"), lax.axis_index("c")

    def copy(self, src, dst, dz=0, dx=0, dy=0, dc=0):
        to = (
            lax.rem(self.z + dz, NZ),
            lax.rem(self.x + dx, NX),
            lax.rem(self.y + dy, NY),
            lax.rem(self.c + dc, NC),
        )
        return self.copy_to(src, dst, to)

    def copy_to(self, src, dst, to):
        made = pltpu.make_async_remote_copy(
            src_ref=src,
            dst_ref=dst,
            send_sem=self.send.at[self.n],
            recv_sem=self.recv.at[self.n],
            device_id=to,
            device_id_type=MESH,
        )
        self.n += 1
        self.all.append(made)
        made.start()
        return made

    def drain(self):
        for made in self.all:
            made.wait_send()


def enter(links):
    z, x, y, c = links.z, links.x, links.y, links.c
    barrier = pltpu.get_barrier_semaphore()
    to = [(dz, 0, 0, 0) for dz in range(1, NZ)]
    to += [(0, dx, dy, 0) for dx, dy in PLANE]
    to += [(0, 0, dy, 1) for dy in range(NY)]
    for dz, dx, dy, dc in to:
        pl.semaphore_signal(
            barrier,
            inc=1,
            device_id=(lax.rem(z + dz, NZ), lax.rem(x + dx, NX), lax.rem(y + dy, NY), lax.rem(c + dc, NC)),
            device_id_type=MESH,
        )
    pl.semaphore_wait(barrier, len(to))


def gather_x_first(links, src, buf):
    z, x, y, c = links.z, links.x, links.y, links.c
    along_x = {dx: links.copy(src, buf.at[x, rows_of(y * NC + c)], dx=dx) for dx in (1, 3, 2)}
    along_y = {}
    for dy in (1, 3, 2):
        along_y[0, dy] = links.copy(src, buf.at[x, rows_of(y * NC + c)], dy=dy)
    forward = [links.copy(src, buf.at[x, rows_of(y * NC + c)], dc=1)]

    def finish():
        def block(dx, dy):
            return buf.at[lax.rem(x - dx + NX, NX), rows_of(lax.rem(y - dy + NY, NY) * NC + c)]

        for dx in (1, 3, 2):
            along_x[dx].wait_recv()
            for dy in (1, 3, 2):
                along_y[dx, dy] = links.copy(block(dx, 0), block(dx, 0), dy=dy)
            forward.append(links.copy(block(dx, 0), block(dx, 0), dc=1))
        for dx in (0, 1, 3, 2):
            for dy in (1, 3, 2):
                along_y[dx, dy].wait_recv()
                forward.append(links.copy(block(dx, dy), block(dx, dy), dc=1))
        for made in forward:
            made.wait_recv()

    return finish


def gather_straight(links, src, buf, rows):
    x, y, c = links.x, links.y, links.c

    def block(xs, ys):
        return buf.at[ys * NC + c, pl.ds(pl.multiple_of(xs * rows, rows), rows)]

    straight = [links.copy(src, block(x, y), dx=dx, dy=dy) for dx, dy in PLANE]
    forward = [links.copy(src, block(x, y), dc=1)]

    def finish():
        for (dx, dy), made in zip(PLANE, straight):
            made.wait_recv()
            came = block(lax.rem(x - dx + NX, NX), lax.rem(y - dy + NY, NY))
            forward.append(links.copy(came, came, dc=1))
        for made in forward:
            made.wait_recv()

    return finish


class RingSum:
    FIRST = ((0, 0, 0), (1, 0, 1), (0, 1, 1), (1, 1, 0))
    LATER = (
        ((0, 1, 0), (1, 1, 1)),
        ((0, 2, 1), (1, 2, 0)),
        ((0, 2, 0), (1, 2, 1)),
        ((0, 3, 1), (1, 3, 0)),
        ((0, 3, 0), (1, 3, 1)),
    )

    def __init__(self, links, block, sendbuf, recvbuf, width):
        self.links, self.block, self.sendbuf, self.recvbuf = links, block, sendbuf, recvbuf
        self.half, self.made = width // 2, {}

    def send(self, way, step, side):
        value = self.block(4 - step if way == 0 else 4 + step)[:, side * self.half : (side + 1) * self.half]
        before = self.made.get((way, step - 1, side))
        if before is not None:
            before.wait_recv()
            value = value + self.recvbuf[way, step - 1, side].astype(F32)
        self.sendbuf[way, step, side] = value.astype(BF)
        self.made[way, step, side] = self.links.copy(
            self.sendbuf.at[way, step, side], self.recvbuf.at[way, step, side], dz=1 if way == 0 else NZ - 1
        )

    def first(self):
        for one in self.FIRST:
            self.send(*one)

    def later(self, number):
        for one in self.LATER[number]:
            self.send(*one)

    def total(self):
        own = self.block(0)
        total = []
        for side in (1, 0):
            for way in (0, 1):
                self.made[way, 3, side].wait_recv()
            total.insert(
                0,
                own[:, side * self.half : (side + 1) * self.half]
                + self.recvbuf[0, 3, side].astype(F32)
                + self.recvbuf[1, 3, side].astype(F32),
            )
        return jnp.concatenate(total, axis=1)


class RingGather:
    def __init__(self, links, buf, rows):
        self.links, self.buf, self.rows, self.going = links, buf, rows // 2, {}

    def piece(self, at, side):
        return self.buf.at[at, pl.ds(side * self.rows, self.rows)]

    def send(self, way, step, side):
        if step:
            self.going[way, step - 1, side].wait_recv()
        block = self.piece(lax.rem(self.links.z + (NZ - step if way == 0 else step), NZ), side)
        self.going[way, step, side] = self.links.copy(block, block, dz=1 if way == 0 else NZ - 1)

    def step(self, step):
        for side in (0, 1):
            for way in (0, 1):
                if step < 3 or side == way:
                    self.send(way, step, side)
        if step == 3:
            for way in (0, 1):
                self.going[way, 2, 1 - way].wait_recv()

    def finish(self):
        for way in (0, 1):
            self.going[way, 3, way].wait_recv()


def square_rows(wide):
    squares = wide * wide
    squares = squares[:, :F] + squares[:, F : 2 * F] + squares[:, 2 * F : 3 * F] + squares[:, 3 * F :]
    if wide.shape[0] < R:
        squares = jnp.concatenate([squares, jnp.zeros((R - wide.shape[0], F), F32)], axis=0)
    ones = jnp.ones((16, F), BF)
    high = squares.astype(BF)
    low = (squares - high.astype(F32)).astype(BF)
    return (dot_t(ones, high) + dot_t(ones, low))[:8]


def stats_total(own, got, made):
    total = own
    for offset in range(1, NZ):
        made[offset].wait_recv()
        total = total + got[offset]
    return jnp.concatenate([total, jnp.zeros((R - 8, R), F32)], axis=0).T


def body(
    x_hbm, len_hbm, state_hbm, gain1_hbm, wq, wk, wv, wo, write_hbm, forget_hbm, rate_hbm, head_gain_hbm, w_out,
    gain2_hbm, w_gate, w_up, w_down,
    out_ref, next_ref,
    xbuf, w4, wr, rate_w, rw, p1, s1, r1, stats1, got1, pre, mine, cols, readings, mixed_own, wz, mz, obuf, orecv,
    hown, hb, stats2, got2, wg, wu, wd, p2, s2, r2, abuf, part, psend, precv, fsend, frecv,
    x_ref, len_ref, state_ref, gain1_ref, write_ref, forget_ref, rate_ref, head_gain_ref, gain2_ref,
    local, send, recv, over_send, over_recv,
):
    links = Links(send, recv)
    z, x, y, c = links.z, links.x, links.y, links.c
    tp = y * NC + c

    locals_ = [pltpu.make_async_copy(w, w4.at[i], local.at[i]) for i, w in enumerate((wq, wk, wv, wo))]

    def window(at):
        return pl.ds(pl.multiple_of((at * 3 - at // (NX - 1)) * F, F), WIN)

    feats = pl.ds(pl.multiple_of(x * F, F), F)
    given = [
        pltpu.make_async_copy(far, near, local.at[11 + i])
        for i, (far, near) in enumerate(
            (
                (x_hbm, x_ref), (write_hbm, write_ref), (forget_hbm, forget_ref), (gain1_hbm, gain1_ref),
                (gain2_hbm, gain2_ref), (len_hbm, len_ref), (rate_hbm, rate_ref), (head_gain_hbm, head_gain_ref),
                (state_hbm, state_ref),
            )
        )
    ]
    for one in given:
        one.start()
    own_x = pltpu.make_async_copy(x_hbm, xbuf.at[x, rows_of(tp)], local.at[4])
    own_out = pltpu.make_async_copy(w_out, wz.at[x], local.at[5])
    own_late = [
        pltpu.make_async_copy(w_gate.at[:, window(x)], wg.at[feats], local.at[6]),
        pltpu.make_async_copy(w_up.at[:, window(x)], wu.at[feats], local.at[7]),
        pltpu.make_async_copy(w_down.at[window(x)], wd.at[x], local.at[8]),
    ]
    for one in locals_ + [own_x, own_out] + own_late:
        one.start()
    for one in given[:8]:
        one.wait()
    small = [write_ref[...].astype(F32), forget_ref[...].astype(F32), jnp.zeros((12, F), F32)]
    rate_w[...] = jnp.concatenate(small, axis=0).astype(BF)
    rw[x] = rate_w[...]
    enter(links)

    finish = gather_x_first(links, x_ref, xbuf)
    for one in locals_:
        one.wait()
    own_w = pltpu.make_async_copy(w4.at[x], wr.at[feats], local.at[9])
    own_w.start()
    early, late, outs = [], [], []
    for dx in (1, 3, 2):
        to = lax.rem(x + dx, NX)
        early.append(links.copy(w4.at[to], wr.at[feats], dx=dx))
        early.append(links.copy(rate_w, rw.at[x], dx=dx))
    for dx in (1, 3, 2):
        outs.append(links.copy(w_out, wz.at[x], dx=dx))
    for dx in (1, 3, 2):
        to = lax.rem(x + dx, NX)
        late.append(links.copy(w_gate.at[:, window(to)], wg.at[feats], dx=dx))
        late.append(links.copy(w_up.at[:, window(to)], wu.at[feats], dx=dx))
    for dx in (1, 3, 2):
        to = lax.rem(x + dx, NX)
        late.append(links.copy(w_down.at[window(to)], wd.at[x], dx=dx))

    which = lax.broadcasted_iota(jnp.int32, (32, F), 0)

    def gain_of(ref):
        wide = ref[...].astype(F32)
        return jnp.concatenate(
            [jnp.sum(jnp.where(which == z * NX + k, wide, 0.0), axis=0, keepdims=True) for k in range(NX)], axis=1
        )

    gain1, gain2 = gain_of(gain1_ref), gain_of(gain2_ref)
    own_x.wait()
    own_w.wait()
    finish()
    for one in early:
        one.wait_recv()

    sub = lax.broadcasted_iota(jnp.int32, (8, R), 0)
    made1, ready = {}, {}

    def projected(offset):
        if offset not in ready:
            ready[offset] = True
            at = rows_of(lax.rem(z + offset, NZ))
            wide = jnp.concatenate([xbuf[k, at, :] for k in range(NX)], axis=1).astype(F32)
            normed = (wide * gain1).astype(BF)
            p1[offset] = jnp.dot(normed, wr[...], preferred_element_type=F32)
            stat = jnp.where(sub == 4, square_rows(wide), 0.0)
            for k in range(NX):
                stat = stat + dot_t(rw[k], normed[:, k * F : (k + 1) * F])[:8]
            stats1[offset] = stat
            if offset:
                made1[offset] = links.copy(stats1.at[offset], got1.at[offset], dz=offset)
        return p1[offset]

    ring = RingSum(links, projected, s1, r1, 256)
    ring.first()
    for number in range(5):
        ring.later(number)
    mine[...] = ring.total().astype(BF)
    quarter = pl.ds(pl.multiple_of(x * 32, 32), 32)
    own_pre = pltpu.make_async_copy(mine.at[quarter], pre.at[x], local.at[10])
    own_pre.start()
    parts = []
    for dx in (2, 1, 3):
        to = lax.rem(x + dx, NX)
        parts.append(links.copy(mine.at[pl.ds(pl.multiple_of(to * 32, 32), 32)], pre.at[x], dx=dx))
    cols[...] = stats_total(stats1[0], got1, made1)
    stat = cols[quarter, :]
    scale = lax.rsqrt(stat[:, 4:5] / D + EPS)
    lane = lax.broadcasted_iota(jnp.int32, (32, R), 1)
    row = lax.broadcasted_iota(jnp.int32, (32, R), 0)
    live = jnp.zeros((32, R), F32)
    for s in range(8):
        inside = (row // NEW == s) & (lax.rem(row, NEW) < len_ref[s])
        live = live + jnp.where(inside, 1.0, 0.0)
    rated = stat * scale
    beta = jax.nn.sigmoid(rated) * live
    rate = jnp.where(lane == 2, rate_ref[0], jnp.where(lane == 3, rate_ref[1], 0.0))
    softplus = jnp.maximum(rated, 0.0) + jnp.log1p(jnp.exp(-jnp.abs(rated)))
    keep = jnp.exp(-rate * softplus * live)
    own_pre.wait()
    for one in parts:
        one.wait_recv()
    given[8].wait()
    query, key, value = (silu(pre[i].astype(F32) * scale) for i in range(3))
    gate = silu(pre[3].astype(F32) * scale)

    def unit(a):
        return a * lax.rsqrt(jnp.sum(a * a, axis=1, keepdims=True) + EPS)

    stacked = []
    for h in range(2):
        at = slice(h * F, (h + 1) * F)
        stacked += [unit(query[:, at]) * F ** (-0.5), unit(key[:, at])]
    turned = jnp.concatenate(stacked, axis=0).T
    for s in range(8):
        for h in range(2):
            state = state_ref[s, h]
            for t in range(NEW):
                r = s * NEW + t
                q_col = turned[:, h * 64 + r : h * 64 + r + 1]
                k_col = turned[:, h * 64 + 32 + r : h * 64 + 33 + r]
                hold = keep[r : r + 1, 2 + h : 3 + h]
                recalled = jnp.sum(k_col * state, axis=0, keepdims=True)
                update = beta[r : r + 1, h : h + 1] * (value[r : r + 1, h * F : (h + 1) * F] - hold * recalled)
                state = hold * state + k_col * update
                readings[r : r + 1, h * F : (h + 1) * F] = jnp.sum(q_col * state, axis=0, keepdims=True)
            next_ref[s, h] = state
    for h in range(2):
        at = slice(h * F, (h + 1) * F)
        read = readings[:, at] * live
        normed = read * lax.rsqrt(jnp.mean(read * read, axis=1, keepdims=True) + EPS)
        mixed_own[:, at] = (normed * head_gain_ref[...] * gate[:, at]).astype(BF)

    along_z = {dz: links.copy(mixed_own, mz.at[z], dz=dz) for dz in (4, 3, 5, 2, 6, 1, 7)}
    mz[z] = mixed_own[...]
    own_out.wait()
    for one in outs:
        one.wait_recv()
    for dz in (1, 7, 2, 6, 3, 5, 4):
        along_z[dz].wait_recv()
    heads = jnp.concatenate([mz[k] for k in range(NZ)], axis=0)
    for k in range(NX):
        terms = jnp.dot(heads, wz[k], preferred_element_type=F32).astype(BF)
        for h in range(2):
            for b in range(NTP):
                obuf[h, b, :, k * F : (k + 1) * F] = terms[b * 32 + h * 16 : b * 32 + h * 16 + 16]
    made = {}
    for h in range(2):
        for k in (4, 3, 5, 2, 6, 1, 7):
            to = lax.rem(tp + k, NTP)
            made[h, k] = links.copy_to(obuf.at[h, to], orecv.at[h, k], (z, x, to // NC, lax.rem(to, NC)))

    finish = []
    for h in range(2):
        attended = obuf[h, tp].astype(F32)
        for k in range(1, NTP):
            made[h, k].wait_recv()
            attended = attended + orecv[h, k].astype(F32)
        at = pl.ds(pl.multiple_of(tp * R + x * 32 + h * 16, 16), 16)
        given = jnp.concatenate([xbuf[k, at, :] for k in range(NX)], axis=1).astype(F32)
        hown[h] = (given + attended).astype(BF)
        hb[h, tp, pl.ds(pl.multiple_of(x * 16, 16), 16), :] = hown[h]
        finish.append(gather_straight(links, hown.at[h], hb.at[h], 16))

    made2, ready2 = ({}, {}), ({}, {})

    def mixer(h):
        def block(offset):
            if offset not in ready2[h]:
                ready2[h][offset] = True
                wide = hb[h, lax.rem(z + offset, NZ)].astype(F32)
                normed = (wide * gain2).astype(BF)
                p2[h, offset, :, :WIN] = jnp.dot(normed, wg[...], preferred_element_type=F32)
                p2[h, offset, :, WIN:] = jnp.dot(normed, wu[...], preferred_element_type=F32)
                stats2[h, offset] = square_rows(wide)
                if offset:
                    made2[h][offset] = links.copy(stats2.at[h, offset], got2.at[h, offset], dz=offset)
            return p2[h, offset]

        return RingSum(links, block, s2.at[h], r2.at[h], 2 * WIN)

    sums = [mixer(h) for h in range(2)]
    gathers = [RingGather(links, abuf.at[h], 64) for h in range(2)]
    odd = lax.rem(z + c, 2)
    partner = (z, x, y, 1 - c)

    def activate(h):
        total = sums[h].total()
        scale2 = lax.rsqrt(stats_total(stats2[h, 0], got2.at[h], made2[h])[:64, 0:1] / D + EPS)
        activated = silu(scale2 * total[:, :WIN]) * (scale2 * total[:, WIN:])
        again = (lax.broadcasted_iota(jnp.int32, (64, WIN), 1) < F) & (x == NX - 1)
        abuf[h, z] = jnp.where(again, 0.0, activated).astype(BF)
        gathers[h].step(0)
        down(h, 0)

    def down(h, offset):
        block = abuf[h, lax.rem(z + offset, NZ)]
        for k in range(NX):
            part[h, offset, :, k * F : (k + 1) * F] = jnp.dot(block, wd[k], preferred_element_type=F32)

    def over(h, base, other):
        at = base + other
        return at, pltpu.make_async_remote_copy(
            src_ref=psend.at[h, at],
            dst_ref=precv.at[h, at],
            send_sem=over_send.at[h, at],
            recv_sem=over_recv.at[h, at],
            device_id=partner,
            device_id_type=MESH,
        )

    def give(h, base):
        at, one = over(h, base, 1 - odd)
        psend[h, at] = part[h, at].astype(BF)
        one.start()

    def gather_step(h, step):
        gathers[h].step(step) if step < 4 else gathers[h].finish()
        if step < 4:
            down(h, NZ - step)
            down(h, step)
        else:
            down(h, 4)
        give(h, (None, 0, 6, 2, 4)[step])

    last = {}

    def spread(h):
        for base in (0, 6, 2, 4):
            at, one = over(h, base, odd)
            one.wait_recv()
            both = (part[h, at] + precv[h, at].astype(F32)).astype(BF)
            to = lax.rem(z + at, NZ) // NC
            for k in range(NX):
                fsend[h, to, k] = both[:, k * F : (k + 1) * F]
        for i, (dx, dy) in enumerate(PLANE):
            last[h, i] = links.copy(
                fsend.at[h, lax.rem(y + dy, NY), lax.rem(x + dx, NX)], frecv.at[h, i], dx=dx, dy=dy
            )

    def put(h):
        result = hb[h, tp, :, feats].astype(F32) + fsend[h, y, x].astype(F32)
        for i in range(len(PLANE)):
            last[h, i].wait_recv()
            result = result + frecv[h, i].astype(F32)
        result = result.astype(BF)
        for k in range(NX):
            out_ref[k * 32 + h * 16 : k * 32 + h * 16 + 16, :] = result[k * 16 : (k + 1) * 16]

    finish[0]()
    for one in own_late:
        one.wait()
    for one in late:
        one.wait_recv()
    sums[0].first()
    finish[1]()
    sums[0].later(0)
    sums[1].first()
    sums[0].later(1)
    sums[0].later(2)
    sums[1].later(0)
    sums[1].later(1)
    sums[0].later(3)
    sums[0].later(4)
    sums[1].later(2)
    sums[1].later(3)
    sums[1].later(4)
    activate(0)
    activate(1)
    gather_step(0, 1)
    gather_step(1, 1)
    gather_step(0, 2)
    gather_step(1, 2)
    gather_step(0, 3)
    gather_step(1, 3)
    gather_step(0, 4)
    spread(0)
    gather_step(1, 4)
    spread(1)
    put(0)
    put(1)
    links.drain()
    for h in range(2):
        for base in (0, 6, 2, 4):
            over(h, base, 1 - odd)[1].wait_send()
    assert links.n <= NSEM, links.n


def local(
    layer_input, seq_lengths, delta_state, attn_gain, w_query, w_key, w_value, w_outgate, w_write, w_forget,
    forget_rate, head_gain, w_out, mixer_gain, w_gate, w_up, w_down,
):
    vmem = pl.BlockSpec(memory_space=pltpu.VMEM)
    hbm = pl.BlockSpec(memory_space=pltpu.HBM)
    scratch = [
        ((NX, NTP * R, F), BF),
        ((4, F, 256), BF),
        ((NX * F, 256), BF),
        ((16, F), BF),
        ((NX, 16, F), BF),
        ((NZ, R, 256), F32),
        ((2, 4, 2, R, 128), BF),
        ((2, 4, 2, R, 128), BF),
        ((NZ, 8, R), F32),
        ((NZ, 8, R), F32),
        ((NX, 32, 256), BF),
        ((R, 256), BF),
        ((R, R), F32),
        ((32, 256), F32),
        ((32, 256), BF),
        ((NX, 256, F), BF),
        ((NZ, 32, 256), BF),
        ((2, NTP, 16, NX * F), BF),
        ((2, NTP, 16, NX * F), BF),
        ((2, 16, NX * F), BF),
        ((2, NTP, 64, NX * F), BF),
        ((2, NZ, 8, R), F32),
        ((2, NZ, 8, R), F32),
        ((NX * F, WIN), BF),
        ((NX * F, WIN), BF),
        ((NX, WIN, F), BF),
        ((2, NZ, 64, 2 * WIN), F32),
        ((2, 2, 4, 2, 64, WIN), BF),
        ((2, 2, 4, 2, 64, WIN), BF),
        ((2, NZ, 64, WIN), BF),
        ((2, NZ, 64, NX * F), F32),
        ((2, NZ, 64, NX * F), BF),
        ((2, NZ, 64, NX * F), BF),
        ((2, NY, NX, 64, F), BF),
        ((2, NX * NY, 64, F), BF),
    ]
    held = [
        pltpu.VMEM((R, F), BF),
        pltpu.SMEM((8,), jnp.int32),
        pltpu.VMEM(delta_state.shape, F32),
        pltpu.VMEM((32, F), BF),
        pltpu.VMEM((2, F), BF),
        pltpu.VMEM((2, F), BF),
        pltpu.SMEM((2,), F32),
        pltpu.VMEM((1, F), F32),
        pltpu.VMEM((32, F), BF),
    ]
    return pl.pallas_call(
        body,
        out_shape=(
            jax.ShapeDtypeStruct((R, F), BF),
            jax.ShapeDtypeStruct(delta_state.shape, F32),
        ),
        in_specs=[
            hbm, hbm, hbm, hbm, hbm, hbm, hbm, hbm, hbm, hbm, hbm, hbm, hbm, hbm, hbm, hbm, hbm,
        ],
        out_specs=(vmem, vmem),
        scratch_shapes=[pltpu.VMEM(shape, dtype) for shape, dtype in scratch]
        + held
        + [
            pltpu.SemaphoreType.DMA((20,)),
            pltpu.SemaphoreType.DMA((NSEM,)),
            pltpu.SemaphoreType.DMA((NSEM,)),
            pltpu.SemaphoreType.DMA((2, NZ)),
            pltpu.SemaphoreType.DMA((2, NZ)),
        ],
        compiler_params=pltpu.CompilerParams(
            collective_id=0, has_side_effects=True, vmem_limit_bytes=VMEM_LIMIT
        ),
    )(
        layer_input, seq_lengths, delta_state, attn_gain.reshape(32, F), w_query, w_key, w_value, w_outgate,
        w_write.T, w_forget.T, forget_rate, head_gain.reshape(1, F), w_out, mixer_gain.reshape(32, F), w_gate, w_up,
        w_down,
    )


def solution(mesh):
    split = Mesh(mesh.devices.reshape(NZ, NX, NY, NC), ("z", "x", "y", "c"))
    kv, tp = ("z", "x"), ("y", "c")
    in_specs = (
        P(tp, kv), P(kv), P(kv, tp, None, None), P(), P(kv, tp), P(kv, tp), P(kv, tp), P(kv, tp), P(kv, tp),
        P(kv, tp), P(tp), P(), P(tp, kv), P(), P(kv, tp), P(kv, tp), P(tp, kv),
    )
    out_specs = (P(tp, kv), P(kv, tp, None, None))
    return jax.shard_map(local, mesh=split, in_specs=in_specs, out_specs=out_specs, check_vma=False)
```

time: 131 us -> 112 us (0.85)
  Pallas kernels: 124 us -> 107 us
  local copies, waits for them, and re-layouts: 5.65 us -> 3.67 us
    pallas_call x1, Pallas kernels: 124 us -> 107 us  [local(): pl.pallas_call(body, out_shape=(jax.ShapeDtypeStruct((R, F), BF), jax.Sha...]
    unnamed x10 -> x2, local copies, waits for them, and re-layouts: 4.34 us -> 3.67 us
where the time goes in v2:
time: 112 us
  Pallas kernels  107 us (96%)
  local copies, waits for them, and re-layouts  3.67 us (3%)
    pallas_call x1, Pallas kernels, local(): pl.pallas_call(body, out_shape=(jax.ShapeDtypeStruct((R, F), BF), jax.Sha...  107 us
    unnamed x2, local copies, waits for them, and re-layouts  3.67 us

profile of v2, /device:TPU:1, one launch (start us, length us, event | category | flops | bytes accessed | tf_op | source)
XLA Modules:
  0.0 111.7 jit_solution(325937143449827147)
XLA Ops:
  0.6 107.4 %shard_map.176 = (bf16[128,128]{1,0:T(8,128)(2,1)}, f32[8,2,128,128]{3,2,1,0:T(8,128)}) custom-call(bf16[128,128]{1,0:T(8,128)(2,1)} %x_hbm.1, s32[8]{0:T(128)} %len_hbm.1, f32[8,2,128,128]{3,2,1,0:T(8,128)} %state_hbm.1, bf16[32,128]{1,0:T(8,128)(2,1)} %bitcast.5, bf16[128,256]{1,0:T(8,128)(2,1)} %wq.1, bf16[128,256]{1,0:T(8,128)(2,1)} %wk.1, ...), custom_call_target="tpu_custom_call" | custom-call | tf_op jit(solution)/shard_map/pallas_call | solution.py:599
  108.1 1.4 %copy.21 = bf16[128,128]{1,0:T(8,128)(2,1)} copy(bf16[128,128]{1,0:T(8,128)(2,1)} %get-tuple-element.4) | data formatting | bytes 65536
  109.4 2.3 %copy.22 = f32[8,2,128,128]{3,2,1,0:T(8,128)} copy(f32[8,2,128,128]{3,2,1,0:T(8,128)} %get-tuple-element.5) | data formatting | bytes 2097152

commit v3 on v2

v3 whole, which is shorter than its diff:
```python
import math

import jax
import jax.numpy as jnp
from jax import lax
from jax.experimental import pallas as pl
from jax.experimental.pallas import tpu as pltpu
from jax.sharding import Mesh
from jax.sharding import PartitionSpec as P

D = 4096
NEW = 4
EPS = 1e-06
NZ, NX, NY, NC = 8, 4, 4, 2
NTP = NY * NC
R = 128
F = 128
WIN = 384
MESH = pl.DeviceIdType.MESH
BF = jnp.bfloat16
F32 = jnp.float32
PLANE = [(dx, dy) for dx in range(NX) for dy in range(NY) if dx or dy]
NRECV = 135
NSEND = 11
VMEM_LIMIT = 58 * 1024 * 1024


def silu(a):
    return a * jax.nn.sigmoid(a)


def rows_of(k):
    return pl.ds(pl.multiple_of(k * R, R), R)


def dot_t(a, b):
    return lax.dot_general(a, b, (((1,), (1,)), ((), ())), preferred_element_type=F32)


class Gate:
    def __init__(self, links):
        self.links, self.index, self.size = links, links.fresh(), 0

    def wait(self):
        self.links.wait_bytes(self.links.recv.at[self.index], self.size)


class Links:
    def __init__(self, send, recv, ruler):
        self.send, self.recv, self.ruler, self.n, self.sent = send, recv, ruler, 0, []
        self.z, self.x = lax.axis_index("z"), lax.axis_index("x")
        self.y, self.c = lax.axis_index("y"), lax.axis_index("c")

    def fresh(self):
        self.n += 1
        return self.n - 1

    def phase(self):
        self.sent.append(0)

    def copy(self, src, dst, dz=0, dx=0, dy=0, dc=0, gate=None):
        to = (
            lax.rem(self.z + dz, NZ),
            lax.rem(self.x + dx, NX),
            lax.rem(self.y + dy, NY),
            lax.rem(self.c + dc, NC),
        )
        return self.copy_to(src, dst, to, gate)

    def copy_to(self, src, dst, to, gate=None, index=None):
        size = math.prod(src.shape) * jnp.dtype(src.dtype).itemsize
        self.sent[-1] += size
        if gate is not None:
            gate.size += size
            index = gate.index
        elif index is None:
            index = self.fresh()
        made = pltpu.make_async_remote_copy(
            src_ref=src,
            dst_ref=dst,
            send_sem=self.send.at[len(self.sent) - 1],
            recv_sem=self.recv.at[index],
            device_id=to,
            device_id_type=MESH,
        )
        made.start()
        return made

    def wait_bytes(self, sem, size):
        part = self.ruler.at[pl.ds(0, size // (2 * F))]
        pltpu.make_async_copy(part, part, sem).wait()

    def drain(self):
        for i, size in enumerate(self.sent):
            self.wait_bytes(self.send.at[i], size)
        assert self.n <= NRECV and len(self.sent) <= NSEND, (self.n, len(self.sent))


def greet(links):
    z, x, y, c = links.z, links.x, links.y, links.c
    barrier = pltpu.get_barrier_semaphore()
    to = [(dz, dx, 0, 0) for dz in (0, 1, NZ - 1) for dx in range(NX) if dz or dx]
    to += [(dz, 0, 0, 0) for dz in range(2, NZ - 1)]
    to += [(0, dx, dy, 0) for dx in range(NX) for dy in range(1, NY)]
    to += [(0, 0, dy, 1) for dy in range(NY)]
    for dz, dx, dy, dc in to:
        pl.semaphore_signal(
            barrier,
            inc=1,
            device_id=(lax.rem(z + dz, NZ), lax.rem(x + dx, NX), lax.rem(y + dy, NY), lax.rem(c + dc, NC)),
            device_id_type=MESH,
        )
    return lambda: pl.semaphore_wait(barrier, len(to))


def gather_x_first(links, src, buf):
    z, x, y, c = links.z, links.x, links.y, links.c
    along_x = {dx: links.copy(src, buf.at[x, rows_of(y * NC + c)], dx=dx) for dx in (1, 3, 2)}
    along_y = {}
    for dy in (1, 3, 2):
        along_y[0, dy] = links.copy(src, buf.at[x, rows_of(y * NC + c)], dy=dy)
    forward = Gate(links)
    links.copy(src, buf.at[x, rows_of(y * NC + c)], dc=1, gate=forward)

    def finish():
        def block(dx, dy):
            return buf.at[lax.rem(x - dx + NX, NX), rows_of(lax.rem(y - dy + NY, NY) * NC + c)]

        for dx in (1, 3, 2):
            along_x[dx].wait_recv()
            for dy in (1, 3, 2):
                along_y[dx, dy] = links.copy(block(dx, 0), block(dx, 0), dy=dy)
            links.copy(block(dx, 0), block(dx, 0), dc=1, gate=forward)
        for dx in (0, 1, 3, 2):
            for dy in (1, 3, 2):
                along_y[dx, dy].wait_recv()
                links.copy(block(dx, dy), block(dx, dy), dc=1, gate=forward)
        forward.wait()

    return finish


def gather_straight(links, src, buf, rows):
    x, y, c = links.x, links.y, links.c

    def block(xs, ys):
        return buf.at[ys * NC + c, pl.ds(pl.multiple_of(xs * rows, rows), rows)]

    straight = [links.copy(src, block(x, y), dx=dx, dy=dy) for dx, dy in PLANE]
    forward = Gate(links)
    links.copy(src, block(x, y), dc=1, gate=forward)

    def finish():
        for (dx, dy), made in zip(PLANE, straight):
            made.wait_recv()
            came = block(lax.rem(x - dx + NX, NX), lax.rem(y - dy + NY, NY))
            links.copy(came, came, dc=1, gate=forward)
        forward.wait()

    return finish


FAR, THREE, TWO, ONE = range(4)


class RingSum:
    FIRST = ((0, FAR, 0), (1, FAR, 1), (0, THREE, 1), (1, THREE, 0), (0, THREE, 0), (1, THREE, 1))
    LATER = (((0, TWO, 1), (1, TWO, 0)), ((0, TWO, 0), (1, TWO, 1)), ((0, ONE, 1), (1, ONE, 0)), ((0, ONE, 0), (1, ONE, 1)))

    def __init__(self, links, block, sendbuf, recvbuf, width):
        self.links, self.block, self.sendbuf, self.recvbuf = links, block, sendbuf, recvbuf
        self.half, self.made = width // 2, {}

    def value(self, way, kind, side):
        value = self.block(4 - kind if way == 0 else 4 + kind)[:, side * self.half : (side + 1) * self.half]
        before = [(way, kind - 1, side)] if kind > THREE else []
        if kind == TWO and side == way:
            before.append((way, FAR, side))
        for one in before:
            self.made[one].wait_recv()
            value = value + self.recvbuf[one].astype(F32)
        return value

    def send(self, way, kind, side):
        at = (way, kind, side)
        self.sendbuf[at] = self.value(*at).astype(BF)
        hops = 2 if kind == FAR else 1
        self.made[at] = self.links.copy(
            self.sendbuf.at[at], self.recvbuf.at[at], dz=hops if way == 0 else NZ - hops
        )

    def first(self):
        for one in self.FIRST:
            self.send(*one)

    def later(self, number):
        for one in self.LATER[number]:
            self.send(*one)

    def total(self):
        own = self.block(0)
        total = []
        for side in (0, 1):
            value = own[:, side * self.half : (side + 1) * self.half]
            for way in (0, 1):
                self.made[way, ONE, side].wait_recv()
                value = value + self.recvbuf[way, ONE, side].astype(F32)
            total.append(value)
        return jnp.concatenate(total, axis=1)


class RingSumWhole:
    def __init__(self, links, block, sendbuf, recvbuf, width):
        self.links, self.block, self.sendbuf, self.recvbuf = links, block, sendbuf, recvbuf
        self.half, self.made = width // 2, {}

    def lanes(self, side):
        return slice(None) if side is None else slice(side * self.half, (side + 1) * self.half)

    def send(self, way, kind, side=None):
        lanes = self.lanes(side)
        value = self.block(4 - kind if way == 0 else 4 + kind)[:, lanes]
        if kind == THREE and side == way:
            self.made[way, FAR, side].wait_recv()
            value = value + self.recvbuf[way, FAR, :, lanes].astype(F32)
        elif kind > THREE:
            for before in ((way, THREE, 1 - way), (way, THREE, way)) if kind == TWO else ((way, TWO, None),):
                self.made[before].wait_recv()
            value = value + self.recvbuf[way, kind - 1].astype(F32)
        self.sendbuf[way, kind, :, lanes] = value.astype(BF)
        at = (way, kind) if side is None else (way, kind, slice(None), pl.ds(side * self.half, self.half))
        self.made[way, kind, side] = self.links.copy(
            self.sendbuf.at[at], self.recvbuf.at[at], dz=1 if way == 0 else NZ - 1
        )

    def first(self):
        for way in (0, 1):
            self.send(way, FAR, way)
        for way in (0, 1):
            self.send(way, THREE, 1 - way)

    def later(self, number):
        for way in (0, 1):
            self.send(way, *((THREE, way), (TWO, None), (ONE, None))[number])

    def total(self):
        value = self.block(0)
        for way in (0, 1):
            self.made[way, ONE, None].wait_recv()
            value = value + self.recvbuf[way, ONE].astype(F32)
        return value


class RingGather:
    def __init__(self, links, buf, rows):
        self.links, self.buf, self.rows, self.going = links, buf, rows // 2, {}

    def step(self, step):
        for way in (0, 1):
            if step:
                self.going[way, step].wait_recv()
            at = lax.rem(self.links.z + (NZ - step if way == 0 else step), NZ)
            if step == 2:
                half = self.buf.at[at, pl.ds(way * self.rows, self.rows)]
                self.going[way, 4] = self.links.copy(half, half, dz=2 if way == 0 else NZ - 2)
            if step < 3:
                self.going[way, step + 1] = self.links.copy(
                    self.buf.at[at], self.buf.at[at], dz=1 if way == 0 else NZ - 1
                )

    def finish(self):
        for way in (0, 1):
            self.going[way, 4].wait_recv()


def square_rows(wide):
    squares = wide * wide
    squares = squares[:, :F] + squares[:, F : 2 * F] + squares[:, 2 * F : 3 * F] + squares[:, 3 * F :]
    if wide.shape[0] < R:
        squares = jnp.concatenate([squares, jnp.zeros((R - wide.shape[0], F), F32)], axis=0)
    ones = jnp.ones((16, F), BF)
    high = squares.astype(BF)
    low = (squares - high.astype(F32)).astype(BF)
    return (dot_t(ones, high) + dot_t(ones, low))[:8]


def stats_total(own, got, gate):
    gate.wait()
    total = own
    for offset in range(1, NZ):
        total = total + got[offset]
    return jnp.concatenate([total, jnp.zeros((R - 8, R), F32)], axis=0).T


def body(
    x_hbm, len_hbm, state_hbm, gain1_hbm, wq, wk, wv, wo, write_hbm, forget_hbm, rate_hbm, head_gain_hbm, w_out,
    gain2_hbm, w_gate, w_up, w_down,
    out_ref, next_hbm,
    xbuf, w4, wr, rate_w, rw, p1, s1, r1, stats1, got1, pre, last1, cols, readings, mixed_own, wz, mz, obuf, orecv,
    hown, hb, stats2, got2, wg, wu, wd, p2, s2, r2, abuf, part, psend, precv, fsend, frecv,
    x_ref, len_ref, state_ref, gain1_ref, write_ref, forget_ref, rate_ref, head_gain_ref, gain2_ref,
    ruler, local, send, recv,
):
    links = Links(send, recv, ruler)
    links.phase()
    arrive = greet(links)
    z, x, y, c = links.z, links.x, links.y, links.c
    tp = y * NC + c

    locals_ = [pltpu.make_async_copy(w, w4.at[i], local.at[i]) for i, w in enumerate((wq, wk, wv, wo))]

    def window(at):
        return pl.ds(pl.multiple_of((at * 3 - at // (NX - 1)) * F, F), WIN)

    feats = pl.ds(pl.multiple_of(x * F, F), F)
    given = [
        pltpu.make_async_copy(far, near, local.at[11 + i])
        for i, (far, near) in enumerate(
            (
                (x_hbm, x_ref), (write_hbm, write_ref), (forget_hbm, forget_ref), (gain1_hbm, gain1_ref),
                (gain2_hbm, gain2_ref), (len_hbm, len_ref), (rate_hbm, rate_ref), (head_gain_hbm, head_gain_ref),
                (state_hbm, state_ref),
            )
        )
    ]
    for one in given:
        one.start()
    own_x = pltpu.make_async_copy(x_hbm, xbuf.at[x, rows_of(tp)], local.at[4])
    own_out = pltpu.make_async_copy(w_out, wz.at[x], local.at[5])
    own_late = [
        pltpu.make_async_copy(w_gate.at[:, window(x)], wg.at[feats], local.at[6]),
        pltpu.make_async_copy(w_up.at[:, window(x)], wu.at[feats], local.at[7]),
        pltpu.make_async_copy(w_down.at[window(x)], wd.at[x], local.at[8]),
    ]
    for one in locals_ + [own_x, own_out] + own_late:
        one.start()
    for one in given[:8]:
        one.wait()
    small = [write_ref[...].astype(F32), forget_ref[...].astype(F32), jnp.zeros((12, F), F32)]
    rate_w[...] = jnp.concatenate(small, axis=0).astype(BF)
    rw[x] = rate_w[...]
    arrive()

    finish = gather_x_first(links, x_ref, xbuf)
    for one in locals_:
        one.wait()
    own_w = pltpu.make_async_copy(w4.at[x], wr.at[feats], local.at[9])
    own_w.start()
    early, early_rates, late, outs = Gate(links), Gate(links), Gate(links), Gate(links)
    for dx in (1, 3, 2):
        to = lax.rem(x + dx, NX)
        links.copy(w4.at[to], wr.at[feats], dx=dx, gate=early)
        links.copy(rate_w, rw.at[x], dx=dx, gate=early_rates)
    links.phase()
    for dx in (1, 3, 2):
        links.copy(w_out, wz.at[x], dx=dx, gate=outs)
    for dx in (1, 3, 2):
        to = lax.rem(x + dx, NX)
        links.copy(w_gate.at[:, window(to)], wg.at[feats], dx=dx, gate=late)
        links.copy(w_up.at[:, window(to)], wu.at[feats], dx=dx, gate=late)
    for dx in (1, 3, 2):
        to = lax.rem(x + dx, NX)
        links.copy(w_down.at[window(to)], wd.at[x], dx=dx, gate=late)
    links.phase()

    which = lax.broadcasted_iota(jnp.int32, (32, F), 0)

    def gain_of(ref):
        wide = ref[...].astype(F32)
        return jnp.concatenate(
            [jnp.sum(jnp.where(which == z * NX + k, wide, 0.0), axis=0, keepdims=True) for k in range(NX)], axis=1
        )

    gain1, gain2 = gain_of(gain1_ref), gain_of(gain2_ref)
    own_x.wait()
    own_w.wait()
    finish()
    early.wait()
    early_rates.wait()
    links.phase()

    sub = lax.broadcasted_iota(jnp.int32, (8, R), 0)
    stats_gate, ready = Gate(links), {}

    def projected(offset):
        if offset not in ready:
            ready[offset] = True
            at = rows_of(lax.rem(z + offset, NZ))
            wide = jnp.concatenate([xbuf[k, at, :] for k in range(NX)], axis=1).astype(F32)
            normed = (wide * gain1).astype(BF)
            p1[offset] = jnp.dot(normed, wr[...], preferred_element_type=F32)
            stat = jnp.where(sub == 4, square_rows(wide), 0.0)
            for k in range(NX):
                stat = stat + dot_t(rw[k], normed[:, k * F : (k + 1) * F])[:8]
            stats1[offset] = stat
            if offset:
                links.copy(stats1.at[offset], got1.at[offset], dz=offset, gate=stats_gate)
        return p1[offset]

    def part_of(at):
        return pl.ds(pl.multiple_of(at * 32, 32), 32)

    ring = RingSum(links, projected, s1, r1, 256)
    ring.first()
    ring.later(0)
    ring.later(1)
    pre_gate = Gate(links)
    last1[2] = projected(0).astype(BF)
    for dx in range(1, NX):
        links.copy(last1.at[2, part_of(lax.rem(x + dx, NX))], pre.at[x, 2], dx=dx, gate=pre_gate)
    for way in (0, 1):
        for side in (1 - way, way):
            last1[way, :, side * F : (side + 1) * F] = ring.value(way, ONE, side).astype(BF)
        for dx in (2, 1, 3, 0):
            links.copy(
                last1.at[way, part_of(lax.rem(x + dx, NX))], pre.at[x, way], dz=1 if way == 0 else NZ - 1, dx=dx,
                gate=pre_gate,
            )
    quarter = part_of(x)
    pre[x, 2] = last1[2, quarter, :]
    cols[...] = stats_total(stats1[0], got1, stats_gate)
    stat = cols[quarter, :]
    scale = lax.rsqrt(stat[:, 4:5] / D + EPS)
    lane = lax.broadcasted_iota(jnp.int32, (32, R), 1)
    row = lax.broadcasted_iota(jnp.int32, (32, R), 0)
    live = jnp.zeros((32, R), F32)
    for s in range(8):
        inside = (row // NEW == s) & (lax.rem(row, NEW) < len_ref[s])
        live = live + jnp.where(inside, 1.0, 0.0)
    rated = stat * scale
    beta = jax.nn.sigmoid(rated) * live
    rate = jnp.where(lane == 2, rate_ref[0], jnp.where(lane == 3, rate_ref[1], 0.0))
    softplus = jnp.maximum(rated, 0.0) + jnp.log1p(jnp.exp(-jnp.abs(rated)))
    keep = jnp.exp(-rate * softplus * live)
    pre_gate.wait()
    links.phase()

    def summed(i):
        return (pre[i, 0].astype(F32) + pre[i, 1].astype(F32) + pre[i, 2].astype(F32)) * scale

    given[8].wait()
    query, key, value, gate = (silu(summed(i)) for i in range(4))

    def unit(a):
        return a * lax.rsqrt(jnp.sum(a * a, axis=1, keepdims=True) + EPS)

    stacked = []
    for h in range(2):
        at = slice(h * F, (h + 1) * F)
        stacked += [unit(query[:, at]) * F ** (-0.5), unit(key[:, at])]
    turned = jnp.concatenate(stacked, axis=0).T
    for s in range(8):
        for h in range(2):
            state = state_ref[s, h]
            for t in range(NEW):
                r = s * NEW + t
                q_col = turned[:, h * 64 + r : h * 64 + r + 1]
                k_col = turned[:, h * 64 + 32 + r : h * 64 + 33 + r]
                hold = keep[r : r + 1, 2 + h : 3 + h]
                recalled = jnp.sum(k_col * state, axis=0, keepdims=True)
                update = beta[r : r + 1, h : h + 1] * (value[r : r + 1, h * F : (h + 1) * F] - hold * recalled)
                state = hold * state + k_col * update
                readings[r : r + 1, h * F : (h + 1) * F] = jnp.sum(q_col * state, axis=0, keepdims=True)
            state_ref[s, h] = state
    for h in range(2):
        at = slice(h * F, (h + 1) * F)
        read = readings[:, at] * live
        normed = read * lax.rsqrt(jnp.mean(read * read, axis=1, keepdims=True) + EPS)
        mixed_own[:, at] = (normed * head_gain_ref[...] * gate[:, at]).astype(BF)

    out_state = pltpu.make_async_copy(state_ref, next_hbm, local.at[10])
    mixed_gate = Gate(links)
    for dz in (4, 3, 5, 2, 6, 1, 7):
        links.copy(mixed_own, mz.at[z], dz=dz, gate=mixed_gate)
    out_state.start()
    mz[z] = mixed_own[...]
    own_out.wait()
    outs.wait()
    mixed_gate.wait()
    heads = jnp.concatenate([mz[k] for k in range(NZ)], axis=0)
    for k in range(NX):
        terms = jnp.dot(heads, wz[k], preferred_element_type=F32).astype(BF)
        for h in range(2):
            for b in range(NTP):
                obuf[h, b, :, k * F : (k + 1) * F] = terms[b * 32 + h * 16 : b * 32 + h * 16 + 16]
    tp_gates = [Gate(links), Gate(links)]
    for h in range(2):
        for k in (4, 3, 5, 2, 6, 1, 7):
            to = lax.rem(tp + k, NTP)
            links.copy_to(obuf.at[h, to], orecv.at[h, k], (z, x, to // NC, lax.rem(to, NC)), tp_gates[h])

    finish = []
    for h in range(2):
        attended = obuf[h, tp].astype(F32)
        links.phase()
        tp_gates[h].wait()
        for k in range(1, NTP):
            attended = attended + orecv[h, k].astype(F32)
        at = pl.ds(pl.multiple_of(tp * R + x * 32 + h * 16, 16), 16)
        given = jnp.concatenate([xbuf[k, at, :] for k in range(NX)], axis=1).astype(F32)
        hown[h] = (given + attended).astype(BF)
        hb[h, tp, pl.ds(pl.multiple_of(x * 16, 16), 16), :] = hown[h]
        finish.append(gather_straight(links, hown.at[h], hb.at[h], 16))

    stats_gates, ready2 = (Gate(links), Gate(links)), ({}, {})

    def mixer(h):
        def block(offset):
            if offset not in ready2[h]:
                ready2[h][offset] = True
                wide = hb[h, lax.rem(z + offset, NZ)].astype(F32)
                normed = (wide * gain2).astype(BF)
                p2[h, offset, :, :WIN] = jnp.dot(normed, wg[...], preferred_element_type=F32)
                p2[h, offset, :, WIN:] = jnp.dot(normed, wu[...], preferred_element_type=F32)
                stats2[h, offset] = square_rows(wide)
                if offset:
                    links.copy(stats2.at[h, offset], got2.at[h, offset], dz=offset, gate=stats_gates[h])
            return p2[h, offset]

        return RingSumWhole(links, block, s2.at[h], r2.at[h], 2 * WIN)

    sums = [mixer(h) for h in range(2)]
    gathers = [RingGather(links, abuf.at[h], 64) for h in range(2)]
    odd = lax.rem(z + c, 2)
    partner = (z, x, y, 1 - c)

    def activate(h):
        total = sums[h].total()
        scale2 = lax.rsqrt(stats_total(stats2[h, 0], got2.at[h], stats_gates[h])[:64, 0:1] / D + EPS)
        activated = silu(scale2 * total[:, :WIN]) * (scale2 * total[:, WIN:])
        again = (lax.broadcasted_iota(jnp.int32, (64, WIN), 1) < F) & (x == NX - 1)
        abuf[h, z] = jnp.where(again, 0.0, activated).astype(BF)
        gathers[h].step(0)
        down(h, 0)

    def down(h, offset):
        block = abuf[h, lax.rem(z + offset, NZ)]
        for k in range(NX):
            part[h, offset, :, k * F : (k + 1) * F] = jnp.dot(block, wd[k], preferred_element_type=F32)

    turns = (0, 6, 2, 4)
    over = {(h, base): links.fresh() for h in range(2) for base in turns}

    def give(h, base):
        at = base + 1 - odd
        psend[h, at] = part[h, at].astype(BF)
        over_made[h, base] = links.copy_to(psend.at[h, at], precv.at[h, at], partner, index=over[h, base])

    over_made = {}

    def gather_step(h, step):
        gathers[h].step(step) if step < 4 else gathers[h].finish()
        if step < 4:
            down(h, NZ - step)
            down(h, step)
        else:
            down(h, 4)
        give(h, turns[step - 1])

    last_gates = [Gate(links), Gate(links)]

    def spread(h):
        links.phase()
        for base in turns:
            at = base + odd
            over_made[h, base].wait_recv()
            both = (part[h, at] + precv[h, at].astype(F32)).astype(BF)
            to = lax.rem(z + at, NZ) // NC
            for k in range(NX):
                fsend[h, to, k] = both[:, k * F : (k + 1) * F]
        for i, (dx, dy) in enumerate(PLANE):
            links.copy(
                fsend.at[h, lax.rem(y + dy, NY), lax.rem(x + dx, NX)], frecv.at[h, i], dx=dx, dy=dy, gate=last_gates[h]
            )

    def put(h):
        result = hb[h, tp, :, feats].astype(F32) + fsend[h, y, x].astype(F32)
        last_gates[h].wait()
        for i in range(len(PLANE)):
            result = result + frecv[h, i].astype(F32)
        result = result.astype(BF)
        for k in range(NX):
            out_ref[k * 32 + h * 16 : k * 32 + h * 16 + 16, :] = result[k * 16 : (k + 1) * 16]

    finish[0]()
    for one in own_late:
        one.wait()
    late.wait()
    links.phase()
    sums[0].first()
    finish[1]()
    sums[1].first()
    sums[0].later(0)
    sums[1].later(0)
    sums[0].later(1)
    sums[1].later(1)
    sums[0].later(2)
    sums[1].later(2)
    links.phase()
    activate(0)
    activate(1)
    gather_step(0, 1)
    gather_step(1, 1)
    gather_step(0, 2)
    gather_step(1, 2)
    gather_step(0, 3)
    gather_step(1, 3)
    gather_step(0, 4)
    spread(0)
    gather_step(1, 4)
    spread(1)
    put(0)
    put(1)
    out_state.wait()
    links.drain()


def hand_over(out_tmp, state_tmp, out_ref, state_out, held_out, held_state, came, went):
    pieces = [(out_tmp, held_out, out_ref)]
    pieces += [(state_tmp.at[i], held_state.at[i], state_out.at[i]) for i in range(8)]
    coming = [pltpu.make_async_copy(a, b, came.at[i]) for i, (a, b, _) in enumerate(pieces)]
    going = [pltpu.make_async_copy(b, c, went.at[i]) for i, (_, b, c) in enumerate(pieces)]
    for one in coming:
        one.start()
    for one, two in zip(coming, going):
        one.wait()
        two.start()
    for two in going:
        two.wait()


def local(
    layer_input, seq_lengths, delta_state, attn_gain, w_query, w_key, w_value, w_outgate, w_write, w_forget,
    forget_rate, head_gain, w_out, mixer_gain, w_gate, w_up, w_down,
):
    vmem = pl.BlockSpec(memory_space=pltpu.VMEM)
    hbm = pl.BlockSpec(memory_space=pltpu.HBM)
    scratch = [
        ((NX, NTP * R, F), BF),
        ((4, F, 256), BF),
        ((NX * F, 256), BF),
        ((16, F), BF),
        ((NX, 16, F), BF),
        ((NZ, R, 256), F32),
        ((2, 4, 2, R, 128), BF),
        ((2, 4, 2, R, 128), BF),
        ((NZ, 8, R), F32),
        ((NZ, 8, R), F32),
        ((NX, 3, 32, 256), BF),
        ((3, R, 256), BF),
        ((R, R), F32),
        ((32, 256), F32),
        ((32, 256), BF),
        ((NX, 256, F), BF),
        ((NZ, 32, 256), BF),
        ((2, NTP, 16, NX * F), BF),
        ((2, NTP, 16, NX * F), BF),
        ((2, 16, NX * F), BF),
        ((2, NTP, 64, NX * F), BF),
        ((2, NZ, 8, R), F32),
        ((2, NZ, 8, R), F32),
        ((NX * F, WIN), BF),
        ((NX * F, WIN), BF),
        ((NX, WIN, F), BF),
        ((2, NZ, 64, 2 * WIN), F32),
        ((2, 2, 4, 64, 2 * WIN), BF),
        ((2, 2, 4, 64, 2 * WIN), BF),
        ((2, NZ, 64, WIN), BF),
        ((2, NZ, 64, NX * F), F32),
        ((2, NZ, 64, NX * F), BF),
        ((2, NZ, 64, NX * F), BF),
        ((2, NY, NX, 64, F), BF),
        ((2, NX * NY, 64, F), BF),
    ]
    held = [
        pltpu.VMEM((R, F), BF),
        pltpu.SMEM((8,), jnp.int32),
        pltpu.VMEM(delta_state.shape, F32),
        pltpu.VMEM((32, F), BF),
        pltpu.VMEM((2, F), BF),
        pltpu.VMEM((2, F), BF),
        pltpu.SMEM((2,), F32),
        pltpu.VMEM((1, F), F32),
        pltpu.VMEM((32, F), BF),
    ]
    out_tmp, state_tmp = pl.pallas_call(
        body,
        out_shape=(
            jax.ShapeDtypeStruct((R, F), BF),
            jax.ShapeDtypeStruct(delta_state.shape, F32),
        ),
        in_specs=[
            hbm, hbm, hbm, hbm, hbm, hbm, hbm, hbm, hbm, hbm, hbm, hbm, hbm, hbm, hbm, hbm, hbm,
        ],
        out_specs=(vmem, hbm),
        scratch_shapes=[pltpu.VMEM(shape, dtype) for shape, dtype in scratch]
        + held
        + [
            pltpu.VMEM((16384, F), BF),
            pltpu.SemaphoreType.DMA((20,)),
            pltpu.SemaphoreType.DMA((NSEND,)),
            pltpu.SemaphoreType.DMA((NRECV,)),
        ],
        compiler_params=pltpu.CompilerParams(
            collective_id=0, has_side_effects=True, vmem_limit_bytes=VMEM_LIMIT
        ),
    )(
        layer_input, seq_lengths, delta_state, attn_gain.reshape(32, F), w_query, w_key, w_value, w_outgate,
        w_write.T, w_forget.T, forget_rate, head_gain.reshape(1, F), w_out, mixer_gain.reshape(32, F), w_gate, w_up,
        w_down,
    )
    return pl.pallas_call(
        hand_over,
        out_shape=(
            jax.ShapeDtypeStruct((R, F), BF),
            jax.ShapeDtypeStruct(delta_state.shape, F32),
        ),
        in_specs=[hbm, hbm],
        out_specs=(hbm, hbm),
        scratch_shapes=[
            pltpu.VMEM((R, F), BF),
            pltpu.VMEM(delta_state.shape, F32),
            pltpu.SemaphoreType.DMA((9,)),
            pltpu.SemaphoreType.DMA((9,)),
        ],
        compiler_params=pltpu.CompilerParams(vmem_limit_bytes=VMEM_LIMIT),
    )(out_tmp, state_tmp)


def solution(mesh):
    split = Mesh(mesh.devices.reshape(NZ, NX, NY, NC), ("z", "x", "y", "c"))
    kv, tp = ("z", "x"), ("y", "c")
    in_specs = (
        P(tp, kv), P(kv), P(kv, tp, None, None), P(), P(kv, tp), P(kv, tp), P(kv, tp), P(kv, tp), P(kv, tp),
        P(kv, tp), P(tp), P(), P(tp, kv), P(), P(kv, tp), P(kv, tp), P(tp, kv),
    )
    out_specs = (P(tp, kv), P(kv, tp, None, None))
    return jax.shard_map(local, mesh=split, in_specs=in_specs, out_specs=out_specs, check_vma=False)
```

time: 112 us -> 103 us (0.920)
  Pallas kernels: 107 us -> 102 us
  local copies, waits for them, and re-layouts: 3.67 us -> 0 us
    pallas_call x1, Pallas kernels: 107 us -> 100 us  [local(): pl.pallas_call(body, out_shape=(jax.ShapeDtypeStruct((R, F), BF), jax.Sha...]
    unnamed x2 -> x0, local copies, waits for them, and re-layouts: 3.67 us -> none
    pallas_call x0 -> x1, Pallas kernels: none -> 2.12 us  [local(): pl.pallas_call(hand_over, out_shape=(jax.ShapeDtypeStruct((R, F), BF), ja...]
where the time goes in v3:
time: 103 us
  Pallas kernels  102 us (99%)
    pallas_call x1, Pallas kernels, local(): pl.pallas_call(body, out_shape=(jax.ShapeDtypeStruct((R, F), BF), jax.Sha...  100 us
    pallas_call x1, Pallas kernels, local(): pl.pallas_call(hand_over, out_shape=(jax.ShapeDtypeStruct((R, F), BF), ja...  2.12 us

profile of v3, /device:TPU:1, one launch (start us, length us, event | category | flops | bytes accessed | tf_op | source)
XLA Modules:
  0.0 103.0 jit_solution(16608101480527326713)
XLA Ops:
  0.6 100.2 %shard_map.176 = (bf16[128,128]{1,0:T(8,128)(2,1)}, f32[8,2,128,128]{3,2,1,0:T(8,128)}) custom-call(bf16[128,128]{1,0:T(8,128)(2,1)} %x_hbm.1, s32[8]{0:T(128)} %len_hbm.1, f32[8,2,128,128]{3,2,1,0:T(8,128)} %state_hbm.1, bf16[32,128]{1,0:T(8,128)(2,1)} %bitcast.5, bf16[128,256]{1,0:T(8,128)(2,1)} %wq.1, bf16[128,256]{1,0:T(8,128)(2,1)} %wk.1, ...), custom_call_target="tpu_custom_call" | custom-call | tf_op jit(solution)/shard_map/pallas_call | solution.py:686
  100.8 2.1 %shard_map.177 = (bf16[128,128]{1,0:T(8,128)(2,1)}, f32[8,2,128,128]{3,2,1,0:T(8,128)}) custom-call(bf16[128,128]{1,0:T(8,128)(2,1)} %get-tuple-element.4.out_tmp, f32[8,2,128,128]{3,2,1,0:T(8,128)} %get-tuple-element.5.state_tmp), custom_call_target="tpu_custom_call" | custom-call | tf_op jit(solution)/shard_map/pallas_call | solution.py:712

commit v4 on v3

--- a/solution.py
+++ b/solution.py
@@ -20,7 +20,7 @@
 BF = jnp.bfloat16
 F32 = jnp.float32
 PLANE = [(dx, dy) for dx in range(NX) for dy in range(NY) if dx or dy]
-NRECV = 135
+NRECV = 109
 NSEND = 11
 VMEM_LIMIT = 58 * 1024 * 1024
 
@@ -93,14 +93,14 @@
     def drain(self):
         for i, size in enumerate(self.sent):
             self.wait_bytes(self.send.at[i], size)
-        assert self.n <= NRECV and len(self.sent) <= NSEND, (self.n, len(self.sent))
+        assert self.n == NRECV and len(self.sent) == NSEND, (self.n, len(self.sent))
 
 
 def greet(links):
     z, x, y, c = links.z, links.x, links.y, links.c
     barrier = pltpu.get_barrier_semaphore()
-    to = [(dz, dx, 0, 0) for dz in (0, 1, NZ - 1) for dx in range(NX) if dz or dx]
-    to += [(dz, 0, 0, 0) for dz in range(2, NZ - 1)]
+    to = [(dz, dx, 0, 0) for dz in (0, 1, 2, NZ - 2, NZ - 1) for dx in range(NX) if dz or dx]
+    to += [(dz, 0, 0, 0) for dz in range(3, NZ - 2)]
     to += [(0, dx, dy, 0) for dx in range(NX) for dy in range(1, NY)]
     to += [(0, 0, dy, 1) for dy in range(NY)]
     for dz, dx, dy, dc in to:
@@ -161,52 +161,6 @@
 
 
 FAR, THREE, TWO, ONE = range(4)
-
-
-class RingSum:
-    FIRST = ((0, FAR, 0), (1, FAR, 1), (0, THREE, 1), (1, THREE, 0), (0, THREE, 0), (1, THREE, 1))
-    LATER = (((0, TWO, 1), (1, TWO, 0)), ((0, TWO, 0), (1, TWO, 1)), ((0, ONE, 1), (1, ONE, 0)), ((0, ONE, 0), (1, ONE, 1)))
-
-    def __init__(self, links, block, sendbuf, recvbuf, width):
-        self.links, self.block, self.sendbuf, self.recvbuf = links, block, sendbuf, recvbuf
-        self.half, self.made = width // 2, {}
-
-    def value(self, way, kind, side):
-        value = self.block(4 - kind if way == 0 else 4 + kind)[:, side * self.half : (side + 1) * self.half]
-        before = [(way, kind - 1, side)] if kind > THREE else []
-        if kind == TWO and side == way:
-            before.append((way, FAR, side))
-        for one in before:
-            self.made[one].wait_recv()
-            value = value + self.recvbuf[one].astype(F32)
-        return value
-
-    def send(self, way, kind, side):
-        at = (way, kind, side)
-        self.sendbuf[at] = self.value(*at).astype(BF)
-        hops = 2 if kind == FAR else 1
-        self.made[at] = self.links.copy(
-            self.sendbuf.at[at], self.recvbuf.at[at], dz=hops if way == 0 else NZ - hops
-        )
-
-    def first(self):
-        for one in self.FIRST:
-            self.send(*one)
-
-    def later(self, number):
-        for one in self.LATER[number]:
-            self.send(*one)
-
-    def total(self):
-        own = self.block(0)
-        total = []
-        for side in (0, 1):
-            value = own[:, side * self.half : (side + 1) * self.half]
-            for way in (0, 1):
-                self.made[way, ONE, side].wait_recv()
-                value = value + self.recvbuf[way, ONE, side].astype(F32)
-            total.append(value)
-        return jnp.concatenate(total, axis=1)
 
 
 class RingSumWhole:
@@ -296,7 +250,7 @@
     x_hbm, len_hbm, state_hbm, gain1_hbm, wq, wk, wv, wo, write_hbm, forget_hbm, rate_hbm, head_gain_hbm, w_out,
     gain2_hbm, w_gate, w_up, w_down,
     out_ref, next_hbm,
-    xbuf, w4, wr, rate_w, rw, p1, s1, r1, stats1, got1, pre, last1, cols, readings, mixed_own, wz, mz, obuf, orecv,
+    xbuf, w4, wr, rate_w, rw, p1, s1, r1, stats1, got1, pre, last1, cols, on_first, updates, decays, readings, mixed_own, wz, mz, obuf, orecv,
     hown, hb, stats2, got2, wg, wu, wd, p2, s2, r2, abuf, part, psend, precv, fsend, frecv,
     x_ref, len_ref, state_ref, gain1_ref, write_ref, forget_ref, rate_ref, head_gain_ref, gain2_ref,
     ruler, local, send, recv,
@@ -358,9 +312,6 @@
         to = lax.rem(x + dx, NX)
         links.copy(w_gate.at[:, window(to)], wg.at[feats], dx=dx, gate=late)
         links.copy(w_up.at[:, window(to)], wu.at[feats], dx=dx, gate=late)
-    for dx in (1, 3, 2):
-        to = lax.rem(x + dx, NX)
-        links.copy(w_down.at[window(to)], wd.at[x], dx=dx, gate=late)
     links.phase()
 
     which = lax.broadcasted_iota(jnp.int32, (32, F), 0)
@@ -400,24 +351,34 @@
     def part_of(at):
         return pl.ds(pl.multiple_of(at * 32, 32), 32)
 
-    ring = RingSum(links, projected, s1, r1, 256)
-    ring.first()
-    ring.later(0)
-    ring.later(1)
+    near = {}
+    for way in (0, 1):
+        side = pl.ds(way * F, F)
+        s1[way, 0, :, way * F : (way + 1) * F] = projected(4)[:, way * F : (way + 1) * F].astype(BF)
+        near[way, 0] = links.copy(s1.at[way, 0, :, side], r1.at[way, 0, :, side], dz=2 if way == 0 else NZ - 2)
+    for way in (0, 1):
+        s1[way, 1] = projected(3 if way == 0 else 5).astype(BF)
+        near[way, 1] = links.copy(s1.at[way, 1], r1.at[way, 1], dz=1 if way == 0 else NZ - 1)
     pre_gate = Gate(links)
-    last1[2] = projected(0).astype(BF)
-    for dx in range(1, NX):
-        links.copy(last1.at[2, part_of(lax.rem(x + dx, NX))], pre.at[x, 2], dx=dx, gate=pre_gate)
+
+    def to_owners(slot, value, dz):
+        last1[slot] = value.astype(BF)
+        for dx in (2, 1, 3, 0):
+            if dx or dz:
+                links.copy(last1.at[slot, part_of(lax.rem(x + dx, NX))], pre.at[x, slot], dz=dz, dx=dx, gate=pre_gate)
+
+    to_owners(1, projected(1), 1)
+    to_owners(2, projected(7), NZ - 1)
+    to_owners(0, projected(0), 0)
     for way in (0, 1):
-        for side in (1 - way, way):
-            last1[way, :, side * F : (side + 1) * F] = ring.value(way, ONE, side).astype(BF)
-        for dx in (2, 1, 3, 0):
-            links.copy(
-                last1.at[way, part_of(lax.rem(x + dx, NX))], pre.at[x, way], dz=1 if way == 0 else NZ - 1, dx=dx,
-                gate=pre_gate,
-            )
+        value = projected(2 if way == 0 else 6)
+        near[way, 0].wait_recv()
+        near[way, 1].wait_recv()
+        half = value[:, way * F : (way + 1) * F] + r1[way, 0, :, way * F : (way + 1) * F].astype(F32)
+        halves = [half, value[:, F:]] if way == 0 else [value[:, :F], half]
+        to_owners(3 + way, jnp.concatenate(halves, axis=1) + r1[way, 1].astype(F32), 2 if way == 0 else NZ - 2)
     quarter = part_of(x)
-    pre[x, 2] = last1[2, quarter, :]
+    pre[x, 0] = last1[0, quarter, :]
     cols[...] = stats_total(stats1[0], got1, stats_gate)
     stat = cols[quarter, :]
     scale = lax.rsqrt(stat[:, 4:5] / D + EPS)
@@ -436,9 +397,12 @@
     links.phase()
 
     def summed(i):
-        return (pre[i, 0].astype(F32) + pre[i, 1].astype(F32) + pre[i, 2].astype(F32)) * scale
+        return sum(pre[i, k].astype(F32) for k in range(5)) * scale
 
     given[8].wait()
+    for dx in (1, 3, 2):
+        to = lax.rem(x + dx, NX)
+        links.copy(w_down.at[window(to)], wd.at[x], dx=dx, gate=late)
     query, key, value, gate = (silu(summed(i)) for i in range(4))
 
     def unit(a):
@@ -448,32 +412,76 @@
     for h in range(2):
         at = slice(h * F, (h + 1) * F)
         stacked += [unit(query[:, at]) * F ** (-0.5), unit(key[:, at])]
-    turned = jnp.concatenate(stacked, axis=0).T
-    for s in range(8):
+    upper = lax.broadcasted_iota(jnp.int32, (8, F), 0) < NEW
+    for pair in range(4):
+        near8 = slice(pair * 8, pair * 8 + 8)
         for h in range(2):
-            state = state_ref[s, h]
-            for t in range(NEW):
-                r = s * NEW + t
-                q_col = turned[:, h * 64 + r : h * 64 + r + 1]
-                k_col = turned[:, h * 64 + 32 + r : h * 64 + 33 + r]
-                hold = keep[r : r + 1, 2 + h : 3 + h]
-                recalled = jnp.sum(k_col * state, axis=0, keepdims=True)
-                update = beta[r : r + 1, h : h + 1] * (value[r : r + 1, h * F : (h + 1) * F] - hold * recalled)
-                state = hold * state + k_col * update
-                readings[r : r + 1, h * F : (h + 1) * F] = jnp.sum(q_col * state, axis=0, keepdims=True)
-            state_ref[s, h] = state
+            both = jnp.concatenate([stacked[2 * h][near8], stacked[2 * h + 1][near8]], axis=0)
+            one, two = (
+                jnp.dot(both, state_ref[2 * pair + i, h], precision=lax.Precision.HIGHEST, preferred_element_type=F32)
+                for i in range(2)
+            )
+            for k in range(2):
+                half = slice(k * 8, k * 8 + 8)
+                on_first[k, near8, h * F : (h + 1) * F] = jnp.where(upper, one[half], two[half])
+    position = lax.rem(row, NEW)
+
+    def later_by(a, n):
+        return jnp.concatenate([a[32 - n :], a[: 32 - n]], axis=0)
+
+    def sooner_by(a, n):
+        return jnp.concatenate([a[n:], a[:n]], axis=0)
+
+    for h in range(2):
+        at = slice(h * F, (h + 1) * F)
+        q_now, k_now, v_now = stacked[2 * h], stacked[2 * h + 1], value[:, at]
+        write = jnp.broadcast_to(beta[:, h : h + 1], (32, F))
+        hold = jnp.broadcast_to(keep[:, 2 + h : 3 + h], (32, F))
+        over1 = hold
+        over2 = over1 * later_by(hold, 1)
+        over3 = over2 * later_by(hold, 2)
+        over4 = over3 * later_by(hold, 3)
+        whole = jnp.where(position == 0, over1, jnp.where(position == 1, over2, jnp.where(position == 2, over3, over4)))
+        alone = write * (v_now - whole * on_first[1, :, at])
+        among_k, among_q = [], [jnp.sum(q_now * k_now, axis=1, keepdims=True)]
+        for n, over_n in ((1, over1), (2, over2), (3, over3)):
+            k_then = later_by(k_now, n)
+            inside = jnp.where(position >= n, over_n, 0.0)
+            among_k.append(write * inside * jnp.sum(k_now * k_then, axis=1, keepdims=True))
+            among_q.append(inside * jnp.sum(q_now * k_then, axis=1, keepdims=True))
+        update = alone
+        for _ in range(NEW - 1):
+            update = alone - sum(among_k[n - 1] * later_by(update, n) for n in (1, 2, 3))
+        reading = whole * on_first[0, :, at] + among_q[0] * update
+        for n in (1, 2, 3):
+            reading = reading + among_q[n] * later_by(update, n)
+        readings[:, at] = reading
+        ahead1 = sooner_by(hold, 1)
+        ahead2 = ahead1 * sooner_by(hold, 2)
+        ahead3 = ahead2 * sooner_by(hold, 3)
+        rest = jnp.where(position == 3, 1.0, jnp.where(position == 2, ahead1, jnp.where(position == 1, ahead2, ahead3)))
+        updates[:, at] = rest * update
+        decays[:, at] = whole
     for h in range(2):
         at = slice(h * F, (h + 1) * F)
         read = readings[:, at] * live
         normed = read * lax.rsqrt(jnp.mean(read * read, axis=1, keepdims=True) + EPS)
         mixed_own[:, at] = (normed * head_gain_ref[...] * gate[:, at]).astype(BF)
 
-    out_state = pltpu.make_async_copy(state_ref, next_hbm, local.at[10])
     mixed_gate = Gate(links)
     for dz in (4, 3, 5, 2, 6, 1, 7):
         links.copy(mixed_own, mz.at[z], dz=dz, gate=mixed_gate)
+    mz[z] = mixed_own[...]
+    turned = jnp.concatenate(stacked, axis=0).T
+    for s in range(8):
+        for h in range(2):
+            at = slice(h * F, (h + 1) * F)
+            state = decays[s * NEW + NEW - 1 : (s + 1) * NEW, at] * state_ref[s, h]
+            for r in range(s * NEW, (s + 1) * NEW):
+                state = state + turned[:, h * 64 + 32 + r : h * 64 + 33 + r] * updates[r : r + 1, at]
+            state_ref[s, h] = state
+    out_state = pltpu.make_async_copy(state_ref, next_hbm, local.at[10])
     out_state.start()
-    mz[z] = mixed_own[...]
     own_out.wait()
     outs.wait()
     mixed_gate.wait()
@@ -642,13 +650,16 @@
         ((16, F), BF),
         ((NX, 16, F), BF),
         ((NZ, R, 256), F32),
-        ((2, 4, 2, R, 128), BF),
-        ((2, 4, 2, R, 128), BF),
+        ((2, 2, R, 256), BF),
+        ((2, 2, R, 256), BF),
         ((NZ, 8, R), F32),
         ((NZ, 8, R), F32),
-        ((NX, 3, 32, 256), BF),
-        ((3, R, 256), BF),
+        ((NX, 5, 32, 256), BF),
+        ((5, R, 256), BF),
         ((R, R), F32),
+        ((2, 32, 256), F32),
+        ((32, 256), F32),
+        ((32, 256), F32),
         ((32, 256), F32),
         ((32, 256), BF),
         ((NX, 256, F), BF),

time: 103 us -> 99.3 us (0.964)
  Pallas kernels: 102 us -> 98.6 us
    pallas_call x1, Pallas kernels: 100 us -> 96.4 us  [local(): pl.pallas_call(body, out_shape=(jax.ShapeDtypeStruct((R, F), BF), jax.Sha...]
where the time goes in v4:
time: 99.3 us; the launch traced here: 99.2 us
  Pallas kernels  98.6 us (99%)
    pallas_call x1, Pallas kernels, local(): pl.pallas_call(body, out_shape=(jax.ShapeDtypeStruct((R, F), BF), jax.Sha...  96.4 us
    pallas_call x1, Pallas kernels, local(): pl.pallas_call(hand_over, out_shape=(jax.ShapeDtypeStruct((R, F), BF), ja...  2.12 us

profile of v4, /device:TPU:1, one launch (start us, length us, event | category | flops | bytes accessed | tf_op | source)
XLA Modules:
  0.0 99.2 jit_solution(12192100139129872064)
XLA Ops:
  0.6 96.4 %shard_map.176 = (bf16[128,128]{1,0:T(8,128)(2,1)}, f32[8,2,128,128]{3,2,1,0:T(8,128)}) custom-call(bf16[128,128]{1,0:T(8,128)(2,1)} %x_hbm.1, s32[8]{0:T(128)} %len_hbm.1, f32[8,2,128,128]{3,2,1,0:T(8,128)} %state_hbm.1, bf16[32,128]{1,0:T(8,128)(2,1)} %bitcast.5, bf16[128,256]{1,0:T(8,128)(2,1)} %wq.1, bf16[128,256]{1,0:T(8,128)(2,1)} %wk.1, ...), custom_call_target="tpu_custom_call" | custom-call | tf_op jit(solution)/shard_map/pallas_call | solution.py:697
  97.1 2.1 %shard_map.177 = (bf16[128,128]{1,0:T(8,128)(2,1)}, f32[8,2,128,128]{3,2,1,0:T(8,128)}) custom-call(bf16[128,128]{1,0:T(8,128)(2,1)} %get-tuple-element.4.out_tmp, f32[8,2,128,128]{3,2,1,0:T(8,128)} %get-tuple-element.5.state_tmp), custom_call_target="tpu_custom_call" | custom-call | tf_op jit(solution)/shard_map/pallas_call | solution.py:723

commit v5 on v4

--- a/solution.py
+++ b/solution.py
@@ -21,7 +21,7 @@
 F32 = jnp.float32
 PLANE = [(dx, dy) for dx in range(NX) for dy in range(NY) if dx or dy]
 NRECV = 109
-NSEND = 11
+NSEND = 10
 VMEM_LIMIT = 58 * 1024 * 1024
 
 
@@ -567,24 +567,33 @@
 
     last_gates = [Gate(links), Gate(links)]
 
-    def spread(h):
-        links.phase()
-        for base in turns:
-            at = base + odd
-            over_made[h, base].wait_recv()
-            both = (part[h, at] + precv[h, at].astype(F32)).astype(BF)
-            to = lax.rem(z + at, NZ) // NC
-            for k in range(NX):
-                fsend[h, to, k] = both[:, k * F : (k + 1) * F]
-        for i, (dx, dy) in enumerate(PLANE):
-            links.copy(
-                fsend.at[h, lax.rem(y + dy, NY), lax.rem(x + dx, NX)], frecv.at[h, i], dx=dx, dy=dy, gate=last_gates[h]
-            )
+    def spread(h, turn):
+        at = turns[turn] + odd
+        over_made[h, turns[turn]].wait_recv()
+        both = (part[h, at] + precv[h, at].astype(F32)).astype(BF)
+        for k in range(NX):
+            fsend[h, turn, k] = both[:, k * F : (k + 1) * F]
+        to = lax.rem(z + at, NZ) // NC
+        for dx in (2, 1, 3):
+            xd = lax.rem(x + dx, NX)
+            links.copy_to(fsend.at[h, turn, xd], frecv.at[h, y * NX + x], (z, xd, to, c), last_gates[h])
+
+        @pl.when(to != y)
+        def _():
+            links.copy_to(fsend.at[h, turn, x], frecv.at[h, y * NX + x], (z, x, to, c), last_gates[h])
+
+        @pl.when(to == y)
+        def _():
+            frecv[h, y * NX + x] = fsend[h, turn, x]
+
+        if turn == 3:
+            links.sent[-1] -= 2 * 64 * F
+            last_gates[h].size -= 2 * 64 * F
 
     def put(h):
-        result = hb[h, tp, :, feats].astype(F32) + fsend[h, y, x].astype(F32)
+        result = hb[h, tp, :, feats].astype(F32)
         last_gates[h].wait()
-        for i in range(len(PLANE)):
+        for i in range(NX * NY):
             result = result + frecv[h, i].astype(F32)
         result = result.astype(BF)
         for k in range(NX):
@@ -607,16 +616,23 @@
     links.phase()
     activate(0)
     activate(1)
+    links.phase()
     gather_step(0, 1)
     gather_step(1, 1)
     gather_step(0, 2)
+    spread(0, 0)
     gather_step(1, 2)
+    spread(1, 0)
     gather_step(0, 3)
+    spread(0, 1)
     gather_step(1, 3)
+    spread(1, 1)
     gather_step(0, 4)
-    spread(0)
+    spread(0, 2)
     gather_step(1, 4)
-    spread(1)
+    spread(1, 2)
+    spread(0, 3)
+    spread(1, 3)
     put(0)
     put(1)
     out_state.wait()

time: 99.3 us -> 96.1 us (0.968)
  Pallas kernels: 98.6 us -> 95.1 us
    pallas_call x1, Pallas kernels: 96.4 us -> 93 us  [local(): pl.pallas_call(body, out_shape=(jax.ShapeDtypeStruct((R, F), BF), jax.Sha...]
where the time goes in v5:
time: 96.1 us; the launch traced here: 95.8 us
  Pallas kernels  95.1 us (99%)
    pallas_call x1, Pallas kernels, local(): pl.pallas_call(body, out_shape=(jax.ShapeDtypeStruct((R, F), BF), jax.Sha...  93 us
    pallas_call x1, Pallas kernels, local(): pl.pallas_call(hand_over, out_shape=(jax.ShapeDtypeStruct((R, F), BF), ja...  2.12 us

profile of v5, /device:TPU:1, one launch (start us, length us, event | category | flops | bytes accessed | tf_op | source)
XLA Modules:
  0.0 95.8 jit_solution(13835112852692502844)
XLA Ops:
  0.6 93.0 %shard_map.176 = (bf16[128,128]{1,0:T(8,128)(2,1)}, f32[8,2,128,128]{3,2,1,0:T(8,128)}) custom-call(bf16[128,128]{1,0:T(8,128)(2,1)} %x_hbm.1, s32[8]{0:T(128)} %len_hbm.1, f32[8,2,128,128]{3,2,1,0:T(8,128)} %state_hbm.1, bf16[32,128]{1,0:T(8,128)(2,1)} %bitcast.5, bf16[128,256]{1,0:T(8,128)(2,1)} %wq.1, bf16[128,256]{1,0:T(8,128)(2,1)} %wk.1, ...), custom_call_target="tpu_custom_call" | custom-call | tf_op jit(solution)/shard_map/pallas_call | solution.py:713
  93.7 2.1 %shard_map.177 = (bf16[128,128]{1,0:T(8,128)(2,1)}, f32[8,2,128,128]{3,2,1,0:T(8,128)}) custom-call(bf16[128,128]{1,0:T(8,128)(2,1)} %get-tuple-element.4.out_tmp, f32[8,2,128,128]{3,2,1,0:T(8,128)} %get-tuple-element.5.state_tmp), custom_call_target="tpu_custom_call" | custom-call | tf_op jit(solution)/shard_map/pallas_call | solution.py:739

commit v6 on v5

--- a/solution.py
+++ b/solution.py
@@ -20,7 +20,8 @@
 BF = jnp.bfloat16
 F32 = jnp.float32
 PLANE = [(dx, dy) for dx in range(NX) for dy in range(NY) if dx or dy]
-NRECV = 109
+STRAIGHT = (False, False)
+NRECV = 110 - 2 * sum(STRAIGHT)
 NSEND = 10
 VMEM_LIMIT = 58 * 1024 * 1024
 
@@ -99,8 +100,8 @@
 def greet(links):
     z, x, y, c = links.z, links.x, links.y, links.c
     barrier = pltpu.get_barrier_semaphore()
-    to = [(dz, dx, 0, 0) for dz in (0, 1, 2, NZ - 2, NZ - 1) for dx in range(NX) if dz or dx]
-    to += [(dz, 0, 0, 0) for dz in range(3, NZ - 2)]
+    to = [(dz, 0, 0, 0) for dz in (4, 3, 5)]
+    to += [(dz, dx, 0, 0) for dz in (2, NZ - 2, 1, NZ - 1, 0) for dx in range(NX) if dz or dx]
     to += [(0, dx, dy, 0) for dx in range(NX) for dy in range(1, NY)]
     to += [(0, 0, dy, 1) for dy in range(NY)]
     for dz, dx, dy, dc in to:
@@ -163,45 +164,56 @@
 FAR, THREE, TWO, ONE = range(4)
 
 
-class RingSumWhole:
-    def __init__(self, links, block, sendbuf, recvbuf, width):
+class RingSum:
+    def __init__(self, links, block, sendbuf, recvbuf, width, straight):
         self.links, self.block, self.sendbuf, self.recvbuf = links, block, sendbuf, recvbuf
-        self.half, self.made = width // 2, {}
+        self.half, self.made, self.straight = width // 2, {}, straight
 
     def lanes(self, side):
         return slice(None) if side is None else slice(side * self.half, (side + 1) * self.half)
+
+    def add(self, value, way, kind, side, lanes):
+        self.made[way, kind, side].wait_recv()
+        return value + self.recvbuf[way, kind, :, lanes].astype(F32)
 
     def send(self, way, kind, side=None):
         lanes = self.lanes(side)
         value = self.block(4 - kind if way == 0 else 4 + kind)[:, lanes]
         if kind == THREE and side == way:
-            self.made[way, FAR, side].wait_recv()
-            value = value + self.recvbuf[way, FAR, :, lanes].astype(F32)
-        elif kind > THREE:
-            for before in ((way, THREE, 1 - way), (way, THREE, way)) if kind == TWO else ((way, TWO, None),):
-                self.made[before].wait_recv()
-            value = value + self.recvbuf[way, kind - 1].astype(F32)
+            value = self.add(value, way, FAR, side, lanes)
+        elif kind == TWO and self.straight:
+            parts = [value[:, : self.half], value[:, self.half :]]
+            parts[way] = self.add(parts[way], way, FAR, way, self.lanes(way))
+            value = self.add(jnp.concatenate(parts, axis=1), way, THREE, None, lanes)
+        elif kind == TWO:
+            self.made[way, THREE, 1 - way].wait_recv()
+            value = self.add(value, way, THREE, way, lanes)
+        elif kind == ONE:
+            value = self.add(value, way, TWO, None, lanes)
         self.sendbuf[way, kind, :, lanes] = value.astype(BF)
         at = (way, kind) if side is None else (way, kind, slice(None), pl.ds(side * self.half, self.half))
+        hops = 2 if kind == FAR and self.straight else 1
         self.made[way, kind, side] = self.links.copy(
-            self.sendbuf.at[at], self.recvbuf.at[at], dz=1 if way == 0 else NZ - 1
+            self.sendbuf.at[at], self.recvbuf.at[at], dz=hops if way == 0 else NZ - hops
         )
 
-    def first(self):
+    def farthest(self):
         for way in (0, 1):
             self.send(way, FAR, way)
+
+    def three(self):
         for way in (0, 1):
-            self.send(way, THREE, 1 - way)
+            self.send(way, THREE, None if self.straight else 1 - way)
 
     def later(self, number):
-        for way in (0, 1):
-            self.send(way, *((THREE, way), (TWO, None), (ONE, None))[number])
+        if number or not self.straight:
+            for way in (0, 1):
+                self.send(way, *((THREE, way), (TWO, None), (ONE, None))[number])
 
     def total(self):
         value = self.block(0)
         for way in (0, 1):
-            self.made[way, ONE, None].wait_recv()
-            value = value + self.recvbuf[way, ONE].astype(F32)
+            value = self.add(value, way, ONE, None, slice(None))
         return value
 
 
@@ -288,14 +300,15 @@
     ]
     for one in locals_ + [own_x, own_out] + own_late:
         one.start()
-    for one in given[:8]:
+    arrive()
+
+    given[0].wait()
+    finish = gather_x_first(links, x_ref, xbuf)
+    for one in given[1:8]:
         one.wait()
     small = [write_ref[...].astype(F32), forget_ref[...].astype(F32), jnp.zeros((12, F), F32)]
     rate_w[...] = jnp.concatenate(small, axis=0).astype(BF)
     rw[x] = rate_w[...]
-    arrive()
-
-    finish = gather_x_first(links, x_ref, xbuf)
     for one in locals_:
         one.wait()
     own_w = pltpu.make_async_copy(w4.at[x], wr.at[feats], local.at[9])
@@ -468,10 +481,11 @@
         normed = read * lax.rsqrt(jnp.mean(read * read, axis=1, keepdims=True) + EPS)
         mixed_own[:, at] = (normed * head_gain_ref[...] * gate[:, at]).astype(BF)
 
-    mixed_gate = Gate(links)
-    for dz in (4, 3, 5, 2, 6, 1, 7):
-        links.copy(mixed_own, mz.at[z], dz=dz, gate=mixed_gate)
-    mz[z] = mixed_own[...]
+    mixed_gates = [Gate(links), Gate(links)]
+    for h in range(2):
+        mz[h, z] = mixed_own[h * 16 : h * 16 + 16, :]
+        for dz in (4, 3, 5, 2, 6, 1, 7):
+            links.copy(mixed_own.at[pl.ds(h * 16, 16)], mz.at[h, z], dz=dz, gate=mixed_gates[h])
     turned = jnp.concatenate(stacked, axis=0).T
     for s in range(8):
         for h in range(2):
@@ -484,15 +498,14 @@
     out_state.start()
     own_out.wait()
     outs.wait()
-    mixed_gate.wait()
-    heads = jnp.concatenate([mz[k] for k in range(NZ)], axis=0)
-    for k in range(NX):
-        terms = jnp.dot(heads, wz[k], preferred_element_type=F32).astype(BF)
-        for h in range(2):
-            for b in range(NTP):
-                obuf[h, b, :, k * F : (k + 1) * F] = terms[b * 32 + h * 16 : b * 32 + h * 16 + 16]
     tp_gates = [Gate(links), Gate(links)]
     for h in range(2):
+        mixed_gates[h].wait()
+        heads = jnp.concatenate([mz[h, k] for k in range(NZ)], axis=0)
+        for k in range(NX):
+            terms = jnp.dot(heads, wz[k], preferred_element_type=F32).astype(BF)
+            for b in range(NTP):
+                obuf[h, b, :, k * F : (k + 1) * F] = terms[b * 16 : b * 16 + 16]
         for k in (4, 3, 5, 2, 6, 1, 7):
             to = lax.rem(tp + k, NTP)
             links.copy_to(obuf.at[h, to], orecv.at[h, k], (z, x, to // NC, lax.rem(to, NC)), tp_gates[h])
@@ -525,7 +538,7 @@
                     links.copy(stats2.at[h, offset], got2.at[h, offset], dz=offset, gate=stats_gates[h])
             return p2[h, offset]
 
-        return RingSumWhole(links, block, s2.at[h], r2.at[h], 2 * WIN)
+        return RingSum(links, block, s2.at[h], r2.at[h], 2 * WIN, STRAIGHT[h])
 
     sums = [mixer(h) for h in range(2)]
     gathers = [RingGather(links, abuf.at[h], 64) for h in range(2)]
@@ -604,10 +617,12 @@
         one.wait()
     late.wait()
     links.phase()
-    sums[0].first()
+    sums[0].farthest()
+    sums[0].three()
     finish[1]()
-    sums[1].first()
+    sums[1].farthest()
     sums[0].later(0)
+    sums[1].three()
     sums[1].later(0)
     sums[0].later(1)
     sums[1].later(1)
@@ -679,7 +694,7 @@
         ((32, 256), F32),
         ((32, 256), BF),
         ((NX, 256, F), BF),
-        ((NZ, 32, 256), BF),
+        ((2, NZ, 16, 256), BF),
         ((2, NTP, 16, NX * F), BF),
         ((2, NTP, 16, NX * F), BF),
         ((2, 16, NX * F), BF),

time: 96.1 us -> 94.2 us (0.980)
  Pallas kernels: 95.1 us -> 93.1 us
    pallas_call x1, Pallas kernels: 93 us -> 91 us  [local(): pl.pallas_call(body, out_shape=(jax.ShapeDtypeStruct((R, F), BF), jax.Sha...]
where the time goes in v6:
time: 94.2 us; the launch traced here: 93.7 us
  Pallas kernels  93.1 us (99%)
    pallas_call x1, Pallas kernels, local(): pl.pallas_call(body, out_shape=(jax.ShapeDtypeStruct((R, F), BF), jax.Sha...  91 us
    pallas_call x1, Pallas kernels, local(): pl.pallas_call(hand_over, out_shape=(jax.ShapeDtypeStruct((R, F), BF), ja...  2.12 us

profile of v6, /device:TPU:1, one launch (start us, length us, event | category | flops | bytes accessed | tf_op | source)
XLA Modules:
  0.0 93.7 jit_solution(11982964936871808771)
XLA Ops:
  0.6 91.0 %shard_map.176 = (bf16[128,128]{1,0:T(8,128)(2,1)}, f32[8,2,128,128]{3,2,1,0:T(8,128)}) custom-call(bf16[128,128]{1,0:T(8,128)(2,1)} %x_hbm.1, s32[8]{0:T(128)} %len_hbm.1, f32[8,2,128,128]{3,2,1,0:T(8,128)} %state_hbm.1, bf16[32,128]{1,0:T(8,128)(2,1)} %bitcast.5, bf16[128,256]{1,0:T(8,128)(2,1)} %wq.1, bf16[128,256]{1,0:T(8,128)(2,1)} %wk.1, ...), custom_call_target="tpu_custom_call" | custom-call | tf_op jit(solution)/shard_map/pallas_call | solution.py:728
  91.6 2.1 %shard_map.177 = (bf16[128,128]{1,0:T(8,128)(2,1)}, f32[8,2,128,128]{3,2,1,0:T(8,128)}) custom-call(bf16[128,128]{1,0:T(8,128)(2,1)} %get-tuple-element.4.out_tmp, f32[8,2,128,128]{3,2,1,0:T(8,128)} %get-tuple-element.5.state_tmp), custom_call_target="tpu_custom_call" | custom-call | tf_op jit(solution)/shard_map/pallas_call | solution.py:754

commit v7 on v6

--- a/solution.py
+++ b/solution.py
@@ -19,9 +19,15 @@
 MESH = pl.DeviceIdType.MESH
 BF = jnp.bfloat16
 F32 = jnp.float32
-PLANE = [(dx, dy) for dx in range(NX) for dy in range(NY) if dx or dy]
+
+
+def hops_of(d):
+    return min(d[0], NX - d[0]) + min(d[1], NY - d[1])
+
+
+PLANE = sorted(((dx, dy) for dx in range(NX) for dy in range(NY) if dx or dy), key=hops_of)
 STRAIGHT = (False, False)
-NRECV = 110 - 2 * sum(STRAIGHT)
+NRECV = 88 - 2 * sum(STRAIGHT)
 NSEND = 10
 VMEM_LIMIT = 58 * 1024 * 1024
 
@@ -147,15 +153,18 @@
     def block(xs, ys):
         return buf.at[ys * NC + c, pl.ds(pl.multiple_of(xs * rows, rows), rows)]
 
-    straight = [links.copy(src, block(x, y), dx=dx, dy=dy) for dx, dy in PLANE]
+    straight = {hops: Gate(links) for hops in range(1, 5)}
+    for d in reversed(PLANE):
+        links.copy(src, block(x, y), dx=d[0], dy=d[1], gate=straight[hops_of(d)])
     forward = Gate(links)
     links.copy(src, block(x, y), dc=1, gate=forward)
 
     def finish():
-        for (dx, dy), made in zip(PLANE, straight):
-            made.wait_recv()
-            came = block(lax.rem(x - dx + NX, NX), lax.rem(y - dy + NY, NY))
-            links.copy(came, came, dc=1, gate=forward)
+        for hops, gate in straight.items():
+            gate.wait()
+            for dx, dy in (d for d in PLANE if hops_of(d) == hops):
+                came = block(lax.rem(x - dx + NX, NX), lax.rem(y - dy + NY, NY))
+                links.copy(came, came, dc=1, gate=forward)
         forward.wait()
 
     return finish

time: 94.2 us -> 94.1 us (level)
  no operation moved by 1% of the time
where the time goes in v7:
time: 94.1 us; the launch traced here: 94 us
  Pallas kernels  93.3 us (99%)
    pallas_call x1, Pallas kernels, local(): pl.pallas_call(body, out_shape=(jax.ShapeDtypeStruct((R, F), BF), jax.Sha...  91.2 us
    pallas_call x1, Pallas kernels, local(): pl.pallas_call(hand_over, out_shape=(jax.ShapeDtypeStruct((R, F), BF), ja...  2.12 us

profile of v7, /device:TPU:1, one launch (start us, length us, event | category | flops | bytes accessed | tf_op | source)
XLA Modules:
  0.0 94.0 jit_solution(8766710496273392483)
XLA Ops:
  0.6 91.2 %shard_map.176 = (bf16[128,128]{1,0:T(8,128)(2,1)}, f32[8,2,128,128]{3,2,1,0:T(8,128)}) custom-call(bf16[128,128]{1,0:T(8,128)(2,1)} %x_hbm.1, s32[8]{0:T(128)} %len_hbm.1, f32[8,2,128,128]{3,2,1,0:T(8,128)} %state_hbm.1, bf16[32,128]{1,0:T(8,128)(2,1)} %bitcast.5, bf16[128,256]{1,0:T(8,128)(2,1)} %wq.1, bf16[128,256]{1,0:T(8,128)(2,1)} %wk.1, ...), custom_call_target="tpu_custom_call" | custom-call | tf_op jit(solution)/shard_map/pallas_call | solution.py:737
  91.9 2.1 %shard_map.177 = (bf16[128,128]{1,0:T(8,128)(2,1)}, f32[8,2,128,128]{3,2,1,0:T(8,128)}) custom-call(bf16[128,128]{1,0:T(8,128)(2,1)} %get-tuple-element.4.out_tmp, f32[8,2,128,128]{3,2,1,0:T(8,128)} %get-tuple-element.5.state_tmp), custom_call_target="tpu_custom_call" | custom-call | tf_op jit(solution)/shard_map/pallas_call | solution.py:763

commit v8 on v7

--- a/solution.py
+++ b/solution.py
@@ -333,7 +333,6 @@
     for dx in (1, 3, 2):
         to = lax.rem(x + dx, NX)
         links.copy(w_gate.at[:, window(to)], wg.at[feats], dx=dx, gate=late)
-        links.copy(w_up.at[:, window(to)], wu.at[feats], dx=dx, gate=late)
     links.phase()
 
     which = lax.broadcasted_iota(jnp.int32, (32, F), 0)
@@ -424,6 +423,7 @@
     given[8].wait()
     for dx in (1, 3, 2):
         to = lax.rem(x + dx, NX)
+        links.copy(w_up.at[:, window(to)], wu.at[feats], dx=dx, gate=late)
         links.copy(w_down.at[window(to)], wd.at[x], dx=dx, gate=late)
     query, key, value, gate = (silu(summed(i)) for i in range(4))
 

time: 94.1 us -> 93.9 us (level)
  no operation moved by 1% of the time
where the time goes in v8:
time: 93.9 us; the launch traced here: 93.8 us
  Pallas kernels  93.1 us (99%)
    pallas_call x1, Pallas kernels, local(): pl.pallas_call(body, out_shape=(jax.ShapeDtypeStruct((R, F), BF), jax.Sha...  91 us
    pallas_call x1, Pallas kernels, local(): pl.pallas_call(hand_over, out_shape=(jax.ShapeDtypeStruct((R, F), BF), ja...  2.12 us

profile of v8, /device:TPU:1, one launch (start us, length us, event | category | flops | bytes accessed | tf_op | source)
XLA Modules:
  0.0 93.8 jit_solution(3626888844577188940)
XLA Ops:
  0.6 91.0 %shard_map.176 = (bf16[128,128]{1,0:T(8,128)(2,1)}, f32[8,2,128,128]{3,2,1,0:T(8,128)}) custom-call(bf16[128,128]{1,0:T(8,128)(2,1)} %x_hbm.1, s32[8]{0:T(128)} %len_hbm.1, f32[8,2,128,128]{3,2,1,0:T(8,128)} %state_hbm.1, bf16[32,128]{1,0:T(8,128)(2,1)} %bitcast.5, bf16[128,256]{1,0:T(8,128)(2,1)} %wq.1, bf16[128,256]{1,0:T(8,128)(2,1)} %wk.1, ...), custom_call_target="tpu_custom_call" | custom-call | tf_op jit(solution)/shard_map/pallas_call | solution.py:737
  91.6 2.1 %shard_map.177 = (bf16[128,128]{1,0:T(8,128)(2,1)}, f32[8,2,128,128]{3,2,1,0:T(8,128)}) custom-call(bf16[128,128]{1,0:T(8,128)(2,1)} %get-tuple-element.4.out_tmp, f32[8,2,128,128]{3,2,1,0:T(8,128)} %get-tuple-element.5.state_tmp), custom_call_target="tpu_custom_call" | custom-call | tf_op jit(solution)/shard_map/pallas_call | solution.py:763
